TPU v7x, 256 devices: a whole 4x4x8 slice. The times are simulated.
256 devices in a mesh: ra: 32 (over z, y), cb: 8 (over x, core).
Axes of the slice: x: 4, y: 4, z: 8, core: 2. Of those that a mesh axis runs over, the one named last changes fastest.
Arguments:
- tokens: bfloat16 [2048, 16384], P('ra'), may hold values from -16 to 16
- norm_gain: float32 [2, 2048], replicated, may hold values from 0.1 to 1.9
- up_weight: float32 [2, 2048, 6144], P(None, 'ra', 'cb'), may hold values from -0.125 to 0.125
- gate_weight: float32 [2, 2048, 6144], P(None, 'ra', 'cb'), may hold values from -0.125 to 0.125
- up_scale: float32 [2, 6144], P(None, 'cb'), may hold values from 0.5 to 2
- gate_scale: float32 [2, 6144], P(None, 'cb'), may hold values from 0.5 to 2
- up_taps: float32 [2, 3, 6144], P(None, None, 'cb'), may hold values from -3 to 3
- gate_taps: float32 [2, 3, 6144], P(None, None, 'cb'), may hold values from -3 to 3
- down_weight: float32 [2, 2048, 6144], P(None, 'ra', 'cb'), may hold values from -0.078125 to 0.078125
- down_scale: float32 [2, 2048], replicated, may hold values from 0.5 to 2
Outputs:
- mixed: bfloat16 [2048, 16384], P('ra')
All inputs are finite; a program needn't handle non-finite values.
Results may differ from a plain program's by a relative error of at most 0.024.
Values may be sent and summed in bfloat16 or wider, within the bound.
A program may use at most 64 MiB of HBM per device.

v0:
```python
import jax
import jax.numpy as jnp
from jax import lax
from jax.sharding import Mesh
from jax.sharding import PartitionSpec as P

RA = ("ra_0", "ra_1")


EPS = 1e-06
RESIDUAL = 0.5


def shifted(value, axis, steps):
    count = lax.axis_size(axis)
    initial, last = (max(0, -steps), min(count, count - steps))
    return lax.ppermute(value, axis, [(source, source + steps) for source in range(initial, last)])


def sent_together(arrays, axis, dim, along):
    ends, at = ([], 0)
    for a in arrays[:-1]:
        at += a.shape[along]
        ends.append(at)
    both = jnp.concatenate(arrays, axis=along)
    return tuple(jnp.split(lax.all_gather(both, axis, axis=dim, tiled=True), ends, axis=along))


def gather_axes(value, axes, dim):
    whole = value
    for number in range(len(axes) - 1, -1, -1):
        whole = lax.all_gather(whole, axes[number], axis=dim, tiled=True)
    return whole


def padded_to(lines, length):
    spare = -len(lines) % length
    return jnp.pad(lines, [(0, spare)] + [(0, 0)] * (lines.ndim - 1))


def total_of(value, axis):
    lines = value.reshape(-1, *value.shape[1:][-1:])
    own = lax.psum_scatter(
        padded_to(lines, lax.axis_size(axis)), axis, scatter_dimension=0, tiled=True
    )
    whole = lax.all_gather(own, axis).reshape(-1, *lines.shape[1:])
    return lax.slice_in_dim(whole, 0, len(lines)).reshape(value.shape)


def valid_taps(values, taps):
    width = taps.shape[0]
    length = values.shape[0] - width + 1
    total = taps[0][None, :] * values[0:length]
    for k in range(1, width):
        total = total + taps[k][None, :] * values[k : k + length]
    return total


def per_device(
    tokens,
    norm_gain,
    up_weight,
    gate_weight,
    up_scale,
    gate_scale,
    up_taps,
    gate_taps,
    down_weight,
    down_scale,
):
    state = lax.all_to_all(tokens, RA, split_axis=1, concat_axis=0, tiled=True).T
    edge = up_taps.shape[1] - 1
    for layer in range(up_weight.shape[0]):
        before = shifted(state[state.shape[0] - edge :], RA, 1)
        rows = jnp.concatenate([before, state], axis=0)
        rows_f = rows.astype(jnp.float32)
        inverse = lax.rsqrt(jnp.mean(rows_f * rows_f, axis=1, keepdims=True) + EPS)
        scaled = (rows_f * norm_gain[layer][None, :]).astype(jnp.bfloat16)
        pieces = sent_together(
            (up_weight[layer].astype(jnp.bfloat16), gate_weight[layer].astype(jnp.bfloat16)),
            RA,
            0,
            1,
        )
        up_raw = jnp.dot(scaled, pieces[0], preferred_element_type=jnp.float32)
        gate_raw = jnp.dot(scaled, pieces[1], preferred_element_type=jnp.float32)
        up_pre = up_raw * inverse * up_scale[layer][None, :]
        gate_pre = gate_raw * inverse * gate_scale[layer][None, :]
        conv_up = valid_taps(up_pre, up_taps[layer])
        conv_gate = valid_taps(gate_pre, gate_taps[layer])
        hidden = (jax.nn.silu(conv_gate) * conv_up).astype(jnp.bfloat16)
        down_part = lax.dot_general(
            hidden,
            gather_axes(down_weight[layer].astype(jnp.bfloat16), RA, 0),
            (((1,), (1,)), ((), ())),
            preferred_element_type=jnp.float32,
        )
        down = total_of(down_part.astype(jnp.bfloat16), "cb").astype(jnp.float32)
        state = (down * down_scale[layer][None, :] + RESIDUAL * state.astype(jnp.float32)).astype(
            jnp.bfloat16
        )
    return lax.all_to_all(state.T, RA, split_axis=0, concat_axis=1, tiled=True)


def solution(mesh):
    torus = Mesh(mesh.devices.reshape(8, 4, mesh.shape["cb"]), ("ra_0", "ra_1", "cb"))
    placed = (
        P(RA, None),
        P(),
        P(None, RA, "cb"),
        P(None, RA, "cb"),
        P(None, "cb"),
        P(None, "cb"),
        P(None, None, "cb"),
        P(None, None, "cb"),
        P(None, RA, "cb"),
        P(),
    )
    return jax.shard_map(
        per_device, mesh=torus, in_specs=placed, out_specs=P(RA, None), check_vma=False
    )
```

profile of v0, /device:TPU:1, one launch (start us, length us, event | category | flops | bytes accessed | tf_op | source)
XLA Modules:
  0.0 511.3 jit_solution(13660260227973896724)
XLA Ops:
  6.5 0.0 all-gather.13.cloned.1.call-start
  6.5 1.2 convert.14
  7.7 1.0 convert.15
  8.8 0.7 pad_maximum_fusion.6
  9.5 0.0 all-gather.13.cloned.1.call-update
  9.5 0.0 copy-done.3
  9.5 1.6 copy.26
  11.1 0.0 copy-start.7
  11.1 12.2 %all-to-all-start = ((bf16[64,32,512]{2,0,1:T(8,128)(2,1)}), bf16[64,32,512]{2,0,1:T(8,128)(2,1)S(1)}, u32[]{:S(2)}, u32[]{:S(2)}) async-start(bf16[64,32,512]{2,0,1:T(8,128)(2,1)} %bitcast.42), calls=%async_computation | async-start | bytes 4194304 | tf_op jit(solution)/shard_map/all_to_all | solution.py:71
  23.3 0.0 all-gather.17.cloned.1.call-start
  23.4 0.0 copy-done.4
  23.4 16.6 %all-gather = bf16[1,256,768]{2,1,0:T(8,128)(2,1)} all-gather(bf16[1,64,768]{2,1,0:T(8,128)(2,1)S(1)} %get-tuple-element.26), channel_id=2, replica_groups=mesh['ra_0'=8,'ra_1'=4,'cb'=8] {'ra_1'}, dimensions={1}, use_global_device_ids=true | all-gather | bytes 491520 | tf_op jit(solution)/shard_map/all_gather | solution.py:32
  40.0 0.0 all-gather.17.cloned.1.call-update
  40.0 0.0 reduce-scatter.3.cloned.1.call-start
  40.1 0.0 copy-done.9
  40.1 0.0 copy-done.5
  40.1 0.0 copy-done.6
  40.2 0.1 slice_reduce_fusion.3
  40.3 0.0 copy-done.7
  40.3 38.9 %all-to-all-done = bf16[64,32,512]{2,0,1:T(8,128)(2,1)S(1)} async-done(((bf16[64,32,512]{2,0,1:T(8,128)(2,1)}), bf16[64,32,512]{2,0,1:T(8,128)(2,1)S(1)}, u32[]{:S(2)}, u32[]{:S(2)}) %all-to-all-start) | async-done | bytes 2097184 | tf_op jit(solution)/shard_map/all_to_all | solution.py:71
  79.2 1.3 copy-done.2
  80.5 3.0 copy.20
  83.5 4.0 collective-permute-start
  87.5 0.0 copy-done.10
  87.5 0.8 collective-permute-done
  88.4 0.8 fusion.1
  89.2 23.7 %all-gather.13.cloned.1.call-done = bf16[2048,1536]{1,0:T(8,128)(2,1)} async-done(((bf16[64,1536]{1,0:T(8,128)(2,1)}), bf16[2048,1536]{1,0:T(8,128)(2,1)}) %all-gather.13.cloned.1.call-update) | async-done | bytes 6291472 | tf_op jit(solution)/shard_map/all_gather | solution.py:26
  112.9 5.2 %multiply_multiply_fusion.3 = f32[514,768]{1,0:T(8,128)} fusion(bf16[2048,1536]{1,0:T(8,128)(2,1)} %all-gather.13.cloned.1.call-done, f32[2048]{0:T(1024)S(1)} %bitcast.50, f32[768]{0:T(1024)S(1)} %get-tuple-element.18, f32[514]{0:T(1024)S(1)} %add_rsqrt_fusion.1, bf16[512,2048]{1,0:T(8,128)(2,1)S(1)} %bitcast.39, bf16[2,2048]{1,0:T(2,128)(2,1)S(1)} %collective-permute-done), kind=kOutput, calls=%fused_computation.35 | convolution fusion | flops 1624009728 | bytes 6843400 | tf_op jit(solution)/shard_map/dot_general | solution.py:86
  118.1 3.1 multiply_multiply_fusion.2
  121.2 35.7 %all-gather.17.cloned.1.call-done = bf16[1,2048,768]{2,1,0:T(8,128)(2,1)} async-done(((bf16[1,256,768]{2,1,0:T(8,128)(2,1)}), bf16[1,2048,768]{2,1,0:T(8,128)(2,1)}) %all-gather.17.cloned.1.call-update) | async-done | bytes 3145744 | tf_op jit(solution)/shard_map/all_gather | solution.py:32
  156.9 8.9 %fusion.20 = bf16[512,2048]{1,0:T(8,128)(2,1)} fusion(bf16[1,2048,768]{2,1,0:T(8,128)(2,1)} %all-gather.17.cloned.1.call-done, f32[514,768]{1,0:T(8,128)} %multiply_multiply_fusion.2, f32[514,768]{1,0:T(8,128)} %multiply_multiply_fusion.3, f32[768]{0:T(1024)S(1)} %get-tuple-element.12, f32[768]{0:T(1024)S(1)} %get-tuple-element.13, ...), kind=kOutput, calls=%fused_computation.26 | convolution fusion | flops 1617952768 | bytes 14698496 | tf_op jit(solution)/shard_map/dot_general | solution.py:92
  165.8 0.0 reduce-scatter.3.cloned.1.call-update
  165.8 0.0 all-gather.19.cloned.1.call-start
  165.8 33.2 %reduce-scatter.3.cloned.1.call-done = bf16[64,2048]{1,0:T(8,128)(2,1)} async-done(((bf16[512,2048]{1,0:T(8,128)(2,1)}), bf16[64,2048]{1,0:T(8,128)(2,1)}) %reduce-scatter.3.cloned.1.call-update) | async-done | bytes 262160 | tf_op jit(solution)/shard_map/reduce_scatter | solution.py:43
  199.1 0.0 all-gather.19.cloned.1.call-update
  199.1 0.0 all-gather.15.cloned.1.call-start
  199.1 0.7 pad_maximum_fusion.7
  199.8 0.0 all-gather.15.cloned.1.call-update
  199.9 0.0 all-gather.21.cloned.1.call-start
  199.9 10.5 %all-gather.3 = bf16[1,256,768]{2,1,0:T(8,128)(2,1)} all-gather(bf16[1,64,768]{2,1,0:T(8,128)(2,1)S(1)} %get-tuple-element.25), channel_id=5, replica_groups=mesh['ra_0'=8,'ra_1'=4,'cb'=8] {'ra_1'}, dimensions={1}, use_global_device_ids=true | all-gather | bytes 491520 | tf_op jit(solution)/shard_map/all_gather | solution.py:32
  210.4 0.0 all-gather.21.cloned.1.call-update
  210.4 0.0 reduce-scatter.5.cloned.1.call-start
  210.4 0.0 copy-done.8
  210.5 19.8 %all-gather.19.cloned.1.call-done = bf16[512,2048]{1,0:T(8,128)(2,1)} async-done(((bf16[64,2048]{1,0:T(8,128)(2,1)}), bf16[512,2048]{1,0:T(8,128)(2,1)}) %all-gather.19.cloned.1.call-update) | async-done | bytes 2097168 | tf_op jit(solution)/shard_map/all_gather | solution.py:46
  230.3 2.5 fusion.7
  232.8 0.0 copy-start
  232.8 3.3 collective-permute-start.1
  236.1 0.6 collective-permute-done.1
  236.7 0.8 fusion.3
  237.6 82.5 %all-gather.15.cloned.1.call-done = bf16[2048,1536]{1,0:T(8,128)(2,1)} async-done(((bf16[64,1536]{1,0:T(8,128)(2,1)}), bf16[2048,1536]{1,0:T(8,128)(2,1)}) %all-gather.15.cloned.1.call-update) | async-done | bytes 6291472 | tf_op jit(solution)/shard_map/all_gather | solution.py:26
  320.1 5.8 %multiply_multiply_fusion.1 = f32[514,768]{1,0:T(8,128)} fusion(bf16[2048,1536]{1,0:T(8,128)(2,1)} %all-gather.15.cloned.1.call-done, f32[2048]{0:T(1024)S(1)} %bitcast.48, f32[768]{0:T(1024)S(1)} %get-tuple-element.17, f32[514]{0:T(1024)S(1)} %add_rsqrt_fusion, bf16[512,2048]{1,0:T(8,128)(2,1)} %copy-done, bf16[2,2048]{1,0:T(2,128)(2,1)S(1)} %collective-permute-done.1), kind=kOutput, calls=%fused_computation.33 | convolution fusion | flops 1624009728 | bytes 6843400 | tf_op jit(solution)/shard_map/dot_general | solution.py:86
  325.9 0.0 copy-done.12
  325.9 3.1 multiply_multiply_fusion
  329.0 35.0 %all-gather.21.cloned.1.call-done = bf16[1,2048,768]{2,1,0:T(8,128)(2,1)} async-done(((bf16[1,256,768]{2,1,0:T(8,128)(2,1)}), bf16[1,2048,768]{2,1,0:T(8,128)(2,1)}) %all-gather.21.cloned.1.call-update) | async-done | bytes 3145744 | tf_op jit(solution)/shard_map/all_gather | solution.py:32
  364.0 8.9 %fusion.23 = bf16[512,2048]{1,0:T(8,128)(2,1)} fusion(bf16[1,2048,768]{2,1,0:T(8,128)(2,1)} %all-gather.21.cloned.1.call-done, f32[514,768]{1,0:T(8,128)} %multiply_multiply_fusion, f32[514,768]{1,0:T(8,128)} %multiply_multiply_fusion.1, f32[768]{0:T(1024)S(1)} %get-tuple-element.15, f32[768]{0:T(1024)S(1)} %get-tuple-element.16, ...), kind=kOutput, calls=%fused_computation.27 | convolution fusion | flops 1617952768 | bytes 14698496 | tf_op jit(solution)/shard_map/dot_general | solution.py:92
  372.9 0.0 reduce-scatter.5.cloned.1.call-update
  372.9 0.0 all-gather.23.cloned.1.call-start
  373.0 33.2 %reduce-scatter.5.cloned.1.call-done = bf16[64,2048]{1,0:T(8,128)(2,1)} async-done(((bf16[512,2048]{1,0:T(8,128)(2,1)}), bf16[64,2048]{1,0:T(8,128)(2,1)}) %reduce-scatter.5.cloned.1.call-update) | async-done | bytes 262160 | tf_op jit(solution)/shard_map/reduce_scatter | solution.py:43
  406.2 0.0 all-gather.23.cloned.1.call-update
  406.2 31.4 %all-gather.23.cloned.1.call-done = bf16[512,2048]{1,0:T(8,128)(2,1)} async-done(((bf16[64,2048]{1,0:T(8,128)(2,1)}), bf16[512,2048]{1,0:T(8,128)(2,1)}) %all-gather.23.cloned.1.call-update) | async-done | bytes 2097168 | tf_op jit(solution)/shard_map/all_gather | solution.py:46
  437.6 3.8 fusion.26
  441.4 2.9 copy.21
  444.3 58.7 %all_to_all.38 = bf16[32,64,512]{2,1,0:T(8,128)(2,1)S(1)} all-to-all(bf16[32,64,512]{2,1,0:T(8,128)(2,1)S(1)} %bitcast.43), channel_id=1, replica_groups=mesh['ra_0'=8,'ra_1'=4,'cb'=8] {'ra_0','ra_1'}, dimensions={0} | all-to-all | bytes 4194304 | tf_op jit(solution)/shard_map/all_to_all | solution.py:102
  503.0 1.5 copy.24
  (25 shorter events, 0.2 us)
Async XLA Ops:
  6.5 3.0 copy-start.3
  6.5 106.4 %all-gather.13.cloned.1.call-start = ((), (), s32[]{:S(2)}) async-start(), calls=%async_computation.4 | async-start | bytes 6488064 | tf_op jit(solution)/shard_map/all_gather | solution.py:26
  11.1 12.2 %copy-start.4 = (f32[2,64,768]{2,1,0:T(8,128)S(1)}, f32[2,64,768]{2,1,0:T(8,128)}, u32[]{:S(2)}) copy-start(f32[2,64,768]{2,1,0:T(8,128)} %param.18) | copy-start | bytes 1179652
  11.1 29.0 %copy-start.9 = (f32[2,768]{1,0:T(2,128)S(1)}, f32[2,768]{1,0:T(2,128)}, u32[]{:S(2)}) copy-start(f32[2,768]{1,0:T(2,128)} %param.15) | copy-start | bytes 18436
  11.1 29.0 %copy-start.5 = (f32[2,3,768]{2,0,1:T(2,128)S(1)}, f32[2,3,768]{2,0,1:T(2,128)}, u32[]{:S(2)}) copy-start(f32[2,3,768]{2,0,1:T(2,128)} %param.16) | copy-start | bytes 55300
  11.1 29.0 %copy-start.6 = (f32[2,3,768]{2,0,1:T(2,128)S(1)}, f32[2,3,768]{2,0,1:T(2,128)}, u32[]{:S(2)}) copy-start(f32[2,3,768]{2,0,1:T(2,128)} %param.17) | copy-start | bytes 55300
  11.1 29.1 %copy-start.7 = (f32[2,2048]{1,0:T(2,128)S(1)}, f32[2,2048]{1,0:T(2,128)}, u32[]{:S(2)}) copy-start(f32[2,2048]{1,0:T(2,128)} %param.11) | copy-start | bytes 49156
  11.1 68.0 %all-to-all-start = ((bf16[64,32,512]{2,0,1:T(8,128)(2,1)}), bf16[64,32,512]{2,0,1:T(8,128)(2,1)S(1)}, u32[]{:S(2)}, u32[]{:S(2)}) async-start(bf16[64,32,512]{2,0,1:T(8,128)(2,1)} %bitcast.42), calls=%async_computation | async-start | bytes 4194304 | tf_op jit(solution)/shard_map/all_to_all | solution.py:71
  23.3 133.6 %all-gather.17.cloned.1.call-start = ((), (), s32[]{:S(2)}) async-start(), calls=%async_computation.8 | async-start | bytes 3538944 | tf_op jit(solution)/shard_map/all_gather | solution.py:32
  40.0 159.0 %reduce-scatter.3.cloned.1.call-start = ((), (), s32[]{:S(2)}) async-start(), calls=%async_computation.5 | async-start | bytes 2359296 | tf_op jit(solution)/shard_map/reduce_scatter | solution.py:43
  79.2 1.3 copy-start.2
  80.5 7.0 %copy-start.10 = (f32[2,768]{1,0:T(2,128)S(1)}, f32[2,768]{1,0:T(2,128)}, u32[]{:S(2)}) copy-start(f32[2,768]{1,0:T(2,128)} %param.14) | copy-start | bytes 18436
  83.5 4.9 collective-permute-start
  112.9 5.2 %copy-start.11 = (bf16[2048,1536]{1,0:T(8,128)(2,1)S(1)}, bf16[2048,1536]{1,0:T(8,128)(2,1)}, u32[]{:S(2)}) copy-start(bf16[2048,1536]{1,0:T(8,128)(2,1)} %all-gather.13.cloned.1.call-done) | copy-start | bytes 18874372
  165.8 44.7 %copy-start.8 = (f32[2,2048]{1,0:T(2,128)S(1)}, f32[2,2048]{1,0:T(2,128)}, u32[]{:S(2)}) copy-start(f32[2,2048]{1,0:T(2,128)} %param.19) | copy-start | bytes 49156
  165.8 64.5 %all-gather.19.cloned.1.call-start = ((), (), s32[]{:S(2)}) async-start(), calls=%async_computation.9 | async-start | bytes 2359296 | tf_op jit(solution)/shard_map/all_gather | solution.py:46
  199.1 121.0 %all-gather.15.cloned.1.call-start = ((), (), s32[]{:S(2)}) async-start(), calls=%async_computation.6 | async-start | bytes 6488064 | tf_op jit(solution)/shard_map/all_gather | solution.py:26
  199.9 164.2 %all-gather.21.cloned.1.call-start = ((), (), s32[]{:S(2)}) async-start(), calls=%async_computation.10 | async-start | bytes 3538944 | tf_op jit(solution)/shard_map/all_gather | solution.py:32
  210.4 195.8 %reduce-scatter.5.cloned.1.call-start = ((), (), s32[]{:S(2)}) async-start(), calls=%async_computation.7 | async-start | bytes 2359296 | tf_op jit(solution)/shard_map/reduce_scatter | solution.py:43
  232.8 3.9 copy-start
  232.8 3.9 collective-permute-start.1
  320.1 5.8 %copy-start.1 = (bf16[512,2048]{1,0:T(8,128)(2,1)S(1)}, bf16[512,2048]{1,0:T(8,128)(2,1)}, u32[]{:S(2)}) copy-start(bf16[512,2048]{1,0:T(8,128)(2,1)} %copy-done) | copy-start | bytes 6291460
  320.1 5.8 %copy-start.12 = (bf16[2048,1536]{1,0:T(8,128)(2,1)S(1)}, bf16[2048,1536]{1,0:T(8,128)(2,1)}, u32[]{:S(2)}) copy-start(bf16[2048,1536]{1,0:T(8,128)(2,1)} %all-gather.15.cloned.1.call-done) | copy-start | bytes 18874372
  372.9 64.7 %all-gather.23.cloned.1.call-start = ((), (), s32[]{:S(2)}) async-start(), calls=%async_computation.11 | async-start | bytes 2359296 | tf_op jit(solution)/shard_map/all_gather | solution.py:46
Sparse Core Ops, SparseCore 0:
  9.9 102.9 all-gather.12
  114.7 42.0 all-gather.16
  165.9 33.1 reduce-scatter.2
  200.8 29.4 all-gather.18
  232.7 87.2 all-gather.14
  321.7 42.2 all-gather.20
  373.1 33.1 reduce-scatter.4
  408.1 29.4 all-gather.22
where the time goes:
time: 513 us; the launch traced here: 511 us
  waiting for transfers between devices  335 us (65%)
  blocking collectives  85.8 us (17%)
  matrix products  34.9 us (7%)
  starting transfers between devices  19.8 us (4%)
  between operations  13.7 us (3%)
  other arithmetic  11.6 us (2%)
  local copies, waits for them, and re-layouts  10.5 us (2%)
    all_gather x2, waiting for transfers between devices, sent_together(): lax.all_gather(both, axis, axis=dim, tiled=True)  106 us
    all_gather x2, waiting for transfers between devices, gather_axes(): whole = lax.all_gather(whole, axes[number], axis=dim, tiled=True)  70.7 us
    reduce_scatter x2, waiting for transfers between devices, total_of(): lax.psum_scatter(padded_to(lines, lax.axis_size(axis)), axis, scatter_dim...  66.4 us
    all_to_all x1, blocking collectives, per_device(): return lax.all_to_all(state.T, RA, split_axis=0, concat_axis=1, tiled=True)  58.7 us
    all_gather x2, waiting for transfers between devices, total_of(): whole = lax.all_gather(own, axis).reshape(-1, *lines.shape[1:])  51.2 us
    all_to_all x1, waiting for transfers between devices, per_device(): lax.all_to_all(tokens, RA, split_axis=1, concat_axis=0, tiled=True)  38.9 us
    all_gather x2, blocking collectives, gather_axes(): whole = lax.all_gather(whole, axes[number], axis=dim, tiled=True)  27.1 us
    dot_general x2, matrix products, per_device(): lax.dot_general(hidden, gather_axes(down_weight[layer].astype(jnp.bfloat1...  17.8 us
  transfers between devices with their start and end apart: 11, of which 11 were waited for; matrix products, arithmetic and copies ran while one was open for 5% of the time, Pallas kernels for 0%

commit v1 on v0

v1 whole, which is shorter than its diff:
```python
import jax
import jax.numpy as jnp
from jax import lax
from jax.experimental import pallas as pl
from jax.experimental.pallas import tpu as pltpu
from jax.sharding import Mesh
from jax.sharding import PartitionSpec as P

MESH = pl.DeviceIdType.MESH
EPS = 1e-06
RESIDUAL = 0.5
NZ, NY, NX = 8, 4, 4
NR = NZ * NY
CHUNKS = 2

ITEMS = [(m, 0, (256, 384, 256)[m % 3], 768) for m in range(6)]
GATHER_KEYS = ("Ay1", "Ay2", "Az1", "Az2", "Az3", "Az4", "Bz1", "Bz2", "Bz3", "Bz4", "By1", "By2")
KEY = {k + d: i for i, (k, d) in enumerate([(k, d) for k in GATHER_KEYS for d in "pm"])}
SHARE_KEYS = {k: i for i, k in enumerate(("X1p", "X1m", "X2p", "X2m", "D0", "D1", "D2", "D3"))}
SUM_KEYS = {k: i for i, k in enumerate(("D", "Ap", "Am", "Bp", "Bm"))}


def default_order():
    gather = []
    for i in range(len(ITEMS)):
        for st in range(7):
            gather.append((i + st, i, st))
    gather.sort()
    slots = [[(ph, i, st) for t, i, st in gather if t == s for ph in "AB"] for s in range(len(ITEMS) + 6)]
    chunks = range(CHUNKS)

    def share(which, st):
        return [("share", which, j, st) for j in chunks]

    def layer(l):
        ug = [("prep", l)]
        for n in range(3):
            ug += [("ug", l, n), ("halo", l, n)]
        dn = [("conv", l)]
        for j in chunks:
            dn += [("down", l, j), ("sum", l, j, 0)]
        return ug, dn

    after = {s: [] for s in range(len(slots))}
    after[0] = [("in", 0)]
    after[2] = [("in", 1)] + share(0, 0)
    after[3] = share(0, 1)
    after[4] = share(0, 2)
    after[5] = share(0, 3)
    ug, dn = layer(0)
    after[7] = ug
    after[8] = dn + [("sum", 0, j, 1) for j in chunks] + [("sum", 0, j, 2) for j in chunks]
    after[9] = [("sum", 0, j, 3) for j in chunks] + share(1, 0) + share(1, 1)
    after[10] = share(1, 2) + share(1, 3)
    ug, dn = layer(1)
    order = []
    for s, slot in enumerate(slots):
        if s == len(slots) - 1:
            order += ug
        order += slot + after[s]
    order += dn
    for st in (1, 2, 3):
        order += [("sum", 1, j, st) for j in chunks]
    order += [("out", 0)]
    for st in range(4):
        order += share(2, st)
    return order


ORDER = default_order()


class Program:
    def __init__(self, refs):
        (
            self.tok, self.w_in, self.gain, self.us, self.gs, self.ut, self.gt, self.ds, self.out,
            self.w, self.s, self.x, self.pre, self.halo, self.hid, self.part, self.rd, self.q,
            self.rh, self.rf, self.fin,
            self.l_sem, self.gs_sem, self.gr_sem, self.is_sem, self.ir_sem, self.ss_sem, self.sr_sem,
            self.us_sem, self.ur_sem, self.hs_sem, self.hr_sem, self.os_sem, self.or_sem,
        ) = refs
        self.zi, self.yi = lax.axis_index("z"), lax.axis_index("y")
        self.xi, self.ci = lax.axis_index("x"), lax.axis_index("c")
        self.ri = self.zi * NY + self.yi
        self.span = NR // CHUNKS
        self.loaded = set()
        self.w_copies = [
            pltpu.make_async_copy(self.w_in.at[m], self.w.at[m, self.zi, self.yi], self.l_sem.at[m])
            for m in range(6)
        ]

    def gather_region(self, i, key, d, recv):
        m, c0, c1, c2 = ITEMS[i]
        sign = 1 if d == "p" else -1
        hop = int(key[2])
        back = hop if recv else hop - 1
        first, second = pl.ds(c0, c1 - c0), pl.ds(c1, c2 - c1)
        z = lax.rem(self.zi - sign * back + NZ, NZ)
        y = lax.rem(self.yi - sign * back + NY, NY)
        half = pl.ds(0 if d == "p" else 32, 32)
        w = self.w.at[m]
        if key[:2] == "Ay":
            return w.at[self.zi, y, half if hop == 2 else slice(None), first]
        if key[:2] == "Az":
            if hop == 4:
                return w.at[z, pl.ds(0 if d == "p" else 2, 2), :, first]
            return w.at[z, :, :, first]
        if key[:2] == "Bz":
            return w.at[z, self.yi, half if hop == 4 else slice(None), second]
        if hop == 2:
            return w.at[pl.ds(0 if d == "p" else 4, 4), y, :, second]
        return w.at[:, y, :, second]

    def step_to(self, link, d):
        if link == "z":
            return {"z": lax.rem(self.zi + (1 if d == "p" else NZ - 1), NZ)}
        if link == "y":
            return {"y": lax.rem(self.yi + (1 if d == "p" else NY - 1), NY)}
        if link == "x":
            return {"x": lax.rem(self.xi + (1 if d == "p" else NX - 1), NX)}
        return {"c": 1 - self.ci}

    @staticmethod
    def remote(src, dst, send, recv, to):
        return pltpu.make_async_remote_copy(
            src_ref=src, dst_ref=dst, send_sem=send, recv_sem=recv, device_id=to, device_id_type=MESH
        )

    def g_copy(self, i, key, d, recv=False):
        region = self.gather_region(i, key, d, recv)
        k = KEY[key + d]
        return self.remote(
            region, region, self.gs_sem.at[i, k], self.gr_sem.at[i, k], self.step_to(key[1], d)
        )

    def g_send(self, i, key):
        for d in "pm":
            self.g_copy(i, key, d).start()

    def g_wait(self, i, key):
        for d in "pm":
            self.g_copy(i, key, d, True).wait_recv()

    def g_forward(self, i, came, goes):
        for d in "pm":
            self.g_copy(i, came, d, True).wait_recv()
            self.g_copy(i, goes, d).start()

    def own_weights(self, i):
        m = ITEMS[i][0]
        if m not in self.loaded:
            self.loaded.add(m)
            self.w_copies[m].wait()

    def A(self, i, st):
        self.own_weights(i)
        if st == 0:
            self.g_send(i, "Ay1")
        elif st == 1:
            self.g_forward(i, "Ay1", "Ay2")
        elif st == 2:
            self.g_wait(i, "Ay2")
            self.g_send(i, "Az1")
        elif st < 6:
            self.g_forward(i, f"Az{st - 2}", f"Az{st - 1}")
        else:
            self.g_wait(i, "Az4")

    def B(self, i, st):
        self.own_weights(i)
        if st == 0:
            self.g_send(i, "Bz1")
        elif st < 4:
            self.g_forward(i, f"Bz{st}", f"Bz{st + 1}")
        elif st == 4:
            self.g_wait(i, "Bz4")
            self.g_send(i, "By1")
        elif st == 5:
            self.g_forward(i, "By1", "By2")
        else:
            self.g_wait(i, "By2")

    def lanes(self, own=True):
        c = self.ci if own else 1 - self.ci
        return pl.ds(pl.multiple_of(c * 256, 256), 256)

    def in_own(self):
        cols = pl.ds(pl.multiple_of(self.ri * 512 + self.ci * 256, 256), 256)
        rows = pl.ds(pl.multiple_of(self.xi * 16, 16), 16)
        return pltpu.make_async_copy(
            self.tok.at[rows, cols], self.s.at[0, self.ri, self.xi, :, self.lanes()], self.l_sem.at[6]
        )

    def in_copy(self, other, recv=False):
        cols = pl.ds(pl.multiple_of(other * 512 + self.ci * 256, 256), 256)
        rows = pl.ds(pl.multiple_of(self.xi * 16, 16), 16)
        lands = other if recv else self.ri
        return self.remote(
            self.tok.at[rows, cols],
            self.s.at[0, lands, self.xi, :, self.lanes()],
            self.is_sem.at[other],
            self.ir_sem.at[lands],
            {"z": other // NY, "y": lax.rem(other, NY)},
        )

    def each_other(self, do):
        def body(k, carry):
            do(lax.rem(self.ri + k, NR))
            return carry

        lax.fori_loop(1, NR, body, 0)

    def in_(self, st):
        if st == 0:
            self.in_own().start()
            self.each_other(lambda o: self.in_copy(o).start())
        else:
            self.in_own().wait()
            self.each_other(lambda o: self.in_copy(o, True).wait_recv())

    def share_copy(self, which, j, key, recv=False):
        r = self.span
        lo, n = j * r, r
        if key[0] == "X":
            sign = 1 if key[2] == "p" else -1
            hop = int(key[1])
            back = hop if recv else hop - 1
            x = lax.rem(self.xi - sign * back + NX, NX)
            if hop == 2:
                n = r // 2
                lo += 0 if key[2] == "p" else n
            lanes, to = self.lanes(), self.step_to("x", key[2])
        else:
            off = {"D0": 0, "D1": NX - 1, "D2": 1, "D3": 2}[key]
            x = lax.rem(self.xi + off, NX)
            lanes, to = self.lanes(not recv), self.step_to("c", "p")
        region = self.s.at[which, pl.ds(lo, n), x, :, lanes]
        k = SHARE_KEYS[key]
        return self.remote(
            region, region, self.ss_sem.at[which, j, k], self.sr_sem.at[which, j, k], to
        )

    def share(self, which, j, st):
        def start(*keys):
            for k in keys:
                self.share_copy(which, j, k).start()

        def wait(*keys):
            for k in keys:
                self.share_copy(which, j, k, True).wait_recv()

        if st == 0:
            start("X1p", "X1m", "D0")
        elif st == 1:
            wait("X1p")
            start("X2p", "D1")
            wait("X1m")
            start("X2m", "D2")
        elif st == 2:
            wait("X2p", "X2m")
            start("D3")
        else:
            wait("D0", "D1", "D2", "D3")

    def prep(self, l):
        def body(k, acc):
            block = self.s[l, pl.ds(k * 4, 4)].reshape(256, 512)
            t = block.T.astype(jnp.float32)
            cols = pl.ds(pl.multiple_of(k * 256, 256), 256)
            self.x[:, cols] = (t * self.gain[l : l + 1, cols]).astype(jnp.bfloat16)
            sq = t * t
            return acc + sq[:, :128] + sq[:, 128:]

        acc = lax.fori_loop(0, 8, body, jnp.zeros((512, 128), jnp.float32))
        mean = jnp.sum(acc, axis=1, keepdims=True) * (1.0 / 2048)
        self.inverse = lax.rsqrt(mean + EPS)

    def ug(self, l, n):
        cols = slice(n * 256, n * 256 + 256)
        for k, scale in ((0, self.us), (1, self.gs)):
            w = self.w[3 * l + k, :, :, :, cols].reshape(2048, 256)
            raw = jnp.dot(self.x[...], w, preferred_element_type=jnp.float32)
            self.pre[k, 8:520, cols] = raw * self.inverse * scale[l : l + 1, cols]

    def halo_copy(self, l, n):
        cols = pl.ds(n * 256, 256)
        wrap = jnp.where(self.yi == NY - 1, 1, 0)
        to = {"z": lax.rem(self.zi + wrap, NZ), "y": lax.rem(self.yi + 1, NY)}
        return self.remote(
            self.pre.at[:, pl.ds(512, 8), cols], self.halo.at[l, :, :, cols],
            self.hs_sem.at[l, n], self.hr_sem.at[l, n], to,
        )

    def conv(self, l):
        for n in range(3):
            self.halo_copy(l, n).wait_recv()
        first = self.ri == 0
        for n in range(6):
            cols = slice(n * 128, n * 128 + 128)
            both = []
            for k, taps in ((0, self.ut), (1, self.gt)):
                before = self.halo[l, k, :, cols]
                self.pre[k, 0:8, cols] = jnp.where(first, jnp.zeros_like(before), before)
                total = taps[l, 0:1, cols] * self.pre[k, 6:518, cols]
                total += taps[l, 1:2, cols] * self.pre[k, 7:519, cols]
                total += taps[l, 2:3, cols] * self.pre[k, 8:520, cols]
                both.append(total)
            up, gate = both
            self.hid[:, cols] = (gate / (1.0 + jnp.exp(-gate)) * up).astype(jnp.bfloat16)
        for n in range(3):
            self.halo_copy(l, n).wait_send()

    def down(self, l, j):
        def body(k, carry):
            z = j * (NZ // CHUNKS) + k
            w = self.w[3 * l + 2, z].reshape(256, 768)
            part = lax.dot_general(
                w, self.hid[...], (((1,), (1,)), ((), ())), preferred_element_type=jnp.float32
            )
            self.part[l, pl.ds(z * NY, NY)] = part.astype(jnp.bfloat16).reshape(NY, 4, 16, 512)
            return carry

        lax.fori_loop(0, NZ // CHUNKS, body, 0)

    def sum_copy(self, l, j, key):
        r = self.span
        h = r // 2
        k = SUM_KEYS[key]
        sems = (self.us_sem.at[l, j, k], self.ur_sem.at[l, j, k])
        if key == "D":
            return self.remote(
                self.part.at[l, pl.ds(j * r, r), :, :, self.lanes(False)],
                self.rd.at[l, pl.ds(j * r, r)], *sems, self.step_to("c", "p"),
            )
        d = key[1]
        if key[0] == "A":
            lo = j * r + (0 if d == "p" else h)
            return self.remote(
                self.q.at[l, pl.ds(lo, h), lax.rem(self.xi + 2, NX)],
                self.rh.at[l, 0 if d == "p" else 1, pl.ds(j * h, h)], *sems, self.step_to("x", d),
            )
        return self.remote(
            self.q.at[l, pl.ds(j * r, r), lax.rem(self.xi + (1 if d == "p" else NX - 1), NX)],
            self.rf.at[l, 0 if d == "p" else 1, pl.ds(j * r, r)], *sems, self.step_to("x", d),
        )

    def sum(self, l, j, st):
        r = self.span
        h = r // 2
        f32 = jnp.float32
        rows = pl.ds(j * r, r)
        if st == 0:
            self.sum_copy(l, j, "D").start()
        elif st == 1:
            self.sum_copy(l, j, "D").wait_recv()
            mine = self.part[l, rows, :, :, self.lanes()].astype(f32)
            self.q[l, rows] = (mine + self.rd[l, rows].astype(f32)).astype(jnp.bfloat16)
            self.sum_copy(l, j, "Ap").start()
            self.sum_copy(l, j, "Am").start()
        elif st == 2:
            for d, key in ((1, "p"), (-1, "m")):
                self.sum_copy(l, j, "A" + key).wait_recv()
                x = lax.rem(self.xi + d + NX, NX)
                part = pl.ds(j * r + (0 if key == "p" else h), h)
                came = self.rh[l, 0 if key == "p" else 1, pl.ds(j * h, h)].astype(f32)
                self.q[l, part, x] = (self.q[l, part, x].astype(f32) + came).astype(jnp.bfloat16)
                self.sum_copy(l, j, "B" + key).start()
        else:
            self.sum_copy(l, j, "Bp").wait_recv()
            self.sum_copy(l, j, "Bm").wait_recv()
            total = self.q[l, rows, self.xi].astype(f32)
            total += self.rf[l, 0, rows].astype(f32) + self.rf[l, 1, rows].astype(f32)
            scale = self.ds[l, rows]
            scale = jnp.concatenate([scale, scale], axis=2)
            old = self.s[l, rows, self.xi, :, self.lanes()].astype(f32)
            new = (total * scale + RESIDUAL * old).astype(jnp.bfloat16)
            if l == 0:
                self.s[1, rows, self.xi, :, self.lanes()] = new
            else:
                self.fin[rows] = new
                self.each_in(j, lambda o: self.out_copy(o).start())

    def out_copy(self, other, recv=False):
        lands = other if recv else self.ri
        return self.remote(
            self.fin.at[other],
            self.s.at[2, lands, self.xi, :, self.lanes()],
            self.os_sem.at[other],
            self.or_sem.at[lands],
            {"z": other // NY, "y": lax.rem(other, NY)},
        )

    def each_in(self, j, do):
        def body(k, carry):
            other = j * self.span + lax.rem(self.ri + k, self.span)

            @pl.when(other != self.ri)
            def _():
                do(other)

            return carry

        lax.fori_loop(0, self.span, body, 0)

    def out_(self, st):
        self.s[2, self.ri, self.xi, :, self.lanes()] = self.fin[self.ri]
        self.each_other(lambda o: self.out_copy(o, True).wait_recv())

    def run(self):
        for c in self.w_copies:
            c.start()
        for event in ORDER:
            name, rest = event[0], event[1:]
            if name == "halo":
                self.halo_copy(*rest).start()
            elif name in ("in", "out"):
                getattr(self, name + "_")(*rest)
            else:
                getattr(self, name)(*rest)
        copy = pltpu.make_async_copy(self.s.at[2], self.out, self.l_sem.at[7])
        copy.start()
        for i in range(len(ITEMS)):
            for k in GATHER_KEYS:
                for d in "pm":
                    self.g_copy(i, k, d).wait_send()
        self.each_other(lambda o: self.in_copy(o).wait_send())
        self.each_other(lambda o: self.out_copy(o).wait_send())
        for j in range(CHUNKS):
            for which in range(3):
                for k in SHARE_KEYS:
                    self.share_copy(which, j, k).wait_send()
            for l in range(2):
                for k in SUM_KEYS:
                    self.sum_copy(l, j, k).wait_send()
        copy.wait()


def kernel(*refs):
    Program(refs).run()


def per_device(
    tokens, norm_gain, up_weight, gate_weight, up_scale, gate_scale, up_taps, gate_taps,
    down_weight, down_scale,
):
    bf16, f32 = jnp.bfloat16, jnp.float32
    w_in = jnp.stack(
        [w[l] for l in range(2) for w in (up_weight, gate_weight, down_weight)]
    ).astype(bf16)
    scale = lax.dynamic_index_in_dim(
        down_scale.reshape(2, NR, NX, 16), lax.axis_index("x"), axis=2, keepdims=False
    )
    scale = jnp.broadcast_to(scale[..., None], (2, NR, 16, 128))
    vmem, hbm = pl.BlockSpec(memory_space=pltpu.VMEM), pl.BlockSpec(memory_space=pl.ANY)
    dma = pltpu.SemaphoreType.DMA
    n = len(ITEMS)
    out = pl.pallas_call(
        kernel,
        out_shape=jax.ShapeDtypeStruct((NR, 4, 16, 512), bf16),
        in_specs=[hbm, hbm] + [vmem] * 6,
        out_specs=hbm,
        scratch_shapes=[
            pltpu.VMEM((6, NZ, NY, 64, 768), bf16),
            pltpu.VMEM((3, NR, 4, 16, 512), bf16),
            pltpu.VMEM((512, 2048), bf16),
            pltpu.VMEM((2, 520, 768), f32),
            pltpu.VMEM((2, 2, 8, 768), f32),
            pltpu.VMEM((512, 768), bf16),
            pltpu.VMEM((2, NR, 4, 16, 512), bf16),
            pltpu.VMEM((2, NR, 4, 16, 256), bf16),
            pltpu.VMEM((2, NR, 4, 16, 256), bf16),
            pltpu.VMEM((2, 2, NR // 2, 16, 256), bf16),
            pltpu.VMEM((2, 2, NR, 16, 256), bf16),
            pltpu.VMEM((NR, 16, 256), bf16),
            dma((8,)),
            dma((n, 24)), dma((n, 24)),
            dma((NR,)), dma((NR,)),
            dma((3, CHUNKS, 8)), dma((3, CHUNKS, 8)),
            dma((2, CHUNKS, 5)), dma((2, CHUNKS, 5)),
            dma((2, 3)), dma((2, 3)),
            dma((NR,)), dma((NR,)),
        ],
        compiler_params=pltpu.CompilerParams(
            has_side_effects=True, vmem_limit_bytes=60 * 2**20
        ),
    )(tokens, w_in, norm_gain, up_scale, gate_scale, up_taps, gate_taps, scale)
    return out.reshape(NR, 64, 512).transpose(1, 0, 2).reshape(64, NR * 512)


def solution(mesh):
    torus = Mesh(mesh.devices.reshape(NZ, NY, NX, 2), ("z", "y", "x", "c"))
    ra, cb = ("z", "y"), ("x", "c")
    placed = (
        P(ra, None),
        P(),
        P(None, ra, cb),
        P(None, ra, cb),
        P(None, cb),
        P(None, cb),
        P(None, None, cb),
        P(None, None, cb),
        P(None, ra, cb),
        P(),
    )
    return jax.shard_map(
        per_device, mesh=torus, in_specs=placed, out_specs=P(ra, None), check_vma=False
    )
```

time: 513 us -> 201 us (0.39)
  waiting for transfers between devices: 335 us -> 0 us
  Pallas kernels: 0 us -> 188 us
  blocking collectives: 85.8 us -> 0 us
  matrix products: 34.9 us -> 0 us
  starting transfers between devices: 19.8 us -> 0 us
  between operations: 13.7 us -> 0.08 us
  other arithmetic: 11.6 us -> 3.06 us
    all_gather x6 -> x0, waiting for transfers between devices: 228 us -> none  [the longest x2 106 us: sent_together(): lax.all_gather(both, axis, axis=dim, tiled=True)]
    pallas_call x0 -> x1, Pallas kernels: none -> 188 us  [per_device(): pl.pallas_call(kernel, out_shape=jax.ShapeDtypeStruct((NR, 4, 16, 512), b...]
    reduce_scatter x2 -> x0, waiting for transfers between devices: 66.4 us -> none  [total_of(): lax.psum_scatter(padded_to(lines, lax.axis_size(axis)), axis, scatter_dim...]
    all_to_all x1 -> x0, blocking collectives: 58.7 us -> none  [per_device(): return lax.all_to_all(state.T, RA, split_axis=0, concat_axis=1, tiled=True)]
    all_to_all x1 -> x0, waiting for transfers between devices: 38.9 us -> none  [per_device(): lax.all_to_all(tokens, RA, split_axis=1, concat_axis=0, tiled=True)]
    dot_general x6 -> x0, matrix products: 34.9 us -> none  [the longest x2 17.8 us: per_device(): lax.dot_general(hidden, gather_axes(down_weight[layer].astype(jnp.bfloat1...]
    all_gather x2 -> x0, blocking collectives: 27.1 us -> none  [gather_axes(): whole = lax.all_gather(whole, axes[number], axis=dim, tiled=True)]
    all_to_all x1 -> x0, starting transfers between devices: 12.2 us -> none  [per_device(): lax.all_to_all(tokens, RA, split_axis=1, concat_axis=0, tiled=True)]
  transfers between devices with their start and end apart: 11 -> 0, of which waited for: 11 -> 0; matrix products, arithmetic and copies ran while one was open for 5% -> 0% of each run, Pallas kernels for 0% -> 0%
where the time goes in v1:
time: 201 us; the launch traced here: 200 us
  Pallas kernels  188 us (94%)
  local copies, waits for them, and re-layouts  8.53 us (4%)
  other arithmetic  3.06 us (2%)
    pallas_call x1, Pallas kernels, per_device(): pl.pallas_call(kernel, out_shape=jax.ShapeDtypeStruct((NR, 4, 16, 512), b...  188 us

profile of v1, /device:TPU:1, one launch (start us, length us, event | category | flops | bytes accessed | tf_op | source)
XLA Modules:
  0.0 200.0 jit_solution(8707170316231592069)
XLA Ops:
  0.0 1.3 copy.14.refs_5_
  1.3 1.3 copy.15.refs_6_
  2.7 0.9 reshape.11
  3.6 1.0 convert.18
  4.6 1.0 convert.19
  5.6 1.0 convert.20
  6.6 1.0 broadcast_in_dim.9.refs_7_
  7.7 0.0 copy-start
  7.7 0.8 copy-done
  8.6 188.4 %shard_map.100 = bf16[32,4,16,512]{3,2,1,0:T(8,128)(2,1)} custom-call(bf16[64,16384]{1,0:T(8,128)(2,1)} %refs_0_.1, bf16[6,64,768]{2,1,0:T(8,128)(2,1)} %copy-done, f32[2,2048]{1,0:T(2,128)} %refs_2_.1, f32[2,768]{1,0:T(2,128)} %refs_3_.1, f32[2,768]{1,0:T(2,128)} %refs_4_.1, f32[2,3,768]{2,1,0:T(4,128)} %copy.14.refs_5_, f32[2,3,768]{2,1,0:T(4,128)} %copy.15.refs_6_, ...), custom_call_target="tpu_custom_call" | custom-call | tf_op jit(solution)/shard_map/pallas_call | solution.py:457
  196.9 3.1 %copy.17 = bf16[32,8,8,512]{3,2,0,1:T(8,128)(2,1)} copy(bf16[32,8,8,512]{3,2,1,0:T(8,128)(2,1)} %bitcast.6) | data formatting | bytes 4194304 | tf_op jit(solution)/shard_map/reshape | solution.py:487
  (7 shorter events, 0.1 us)
Async XLA Ops:
  7.7 0.8 copy-start

commit v2 on v1

v2 whole, which is shorter than its diff:
```python
import jax
import jax.numpy as jnp
from jax import lax
from jax.experimental import pallas as pl
from jax.experimental.pallas import tpu as pltpu
from jax.sharding import Mesh
from jax.sharding import PartitionSpec as P

MESH = pl.DeviceIdType.MESH
EPS = 1e-06
RESIDUAL = 0.5
NZ, NY, NX = 8, 4, 4
NR = NZ * NY

ITEMS = [(0, 0, 384, 768), (1, 0, 256, 768), (2, 0, 256, 768), (3, 0, 384, 768), (4, 0, 256, 768), (5, 0, 256, 768)]
PAIR_KEYS = ("Ay1", "Ay2", "Az1", "Az2", "Az3", "Az4", "Bz1", "Bz2", "Bz3", "Bz4")
KEY = {k + d: i for i, (k, d) in enumerate([(k, d) for k in PAIR_KEYS for d in "pm"])}
for _k, _name in enumerate(("By1", "By2")):
    for _slot in range(NZ):
        for _d in range(2):
            KEY[_name + "pm"[_d], _slot] = 20 + 16 * _k + 2 * _slot + _d
SHARE_KEYS = {k: i for i, k in enumerate(("X1p", "X1m", "X2p", "X2m", "D0", "D1", "D2", "D3"))}
SUM_KEYS = {k: i for i, k in enumerate(("D", "Ap", "Am", "Bp", "Bm"))}

NEAR = ((0, 4), (4, 8), (12, 8), (20, 8), (28, 4))
HALVES = ((0, 16), (16, 16))
SHARE_CHUNKS = (HALVES, HALVES, NEAR)
SUM_CHUNKS = (HALVES, NEAR)


def offset(slot):
    return (slot + 1) // 2 * (2 * (slot % 2) - 1)


def slots_at(distance):
    return (0,) if distance == 0 else (7,) if distance == 4 else (2 * distance - 1, 2 * distance)


def opposite(slot):
    return slot if slot in (0, 7) else slot + 1 if slot % 2 else slot - 1


ORDER = [
    ("A", 2, 0), ("B", 1, 0), ("B", 3, 0), ("B", 5, 0), ("B", 2, 0), ("A", 0, 0), ("A", 1, 0),
    ("in", 0), ("A", 2, 1), ("A", 3, 0), ("A", 1, 1), ("B", 2, 1), ("B", 4, 0), ("A", 3, 1),
    ("B", 0, 0), ("A", 0, 1), ("A", 1, 2), ("A", 2, 2), ("B", 0, 1), ("B", 1, 1), ("in", 1),
    ("share", 0, 1, 0), ("A", 0, 2), ("B", 2, 2), ("B", 1, 2), ("B", 0, 2), ("A", 1, 3),
    ("C", 1, 1), ("A", 0, 3), ("A", 4, 0), ("B", 3, 1), ("B", 0, 3), ("C", 1, 0), ("A", 4, 1),
    ("C", 1, 2), ("C", 0, 1), ("B", 1, 3), ("share", 0, 0, 0), ("B", 4, 1), ("share", 0, 1, 1),
    ("A", 0, 4), ("B", 0, 4), ("A", 1, 4), ("A", 2, 3), ("share", 0, 1, 2), ("C", 0, 2),
    ("share", 0, 1, 3), ("C", 0, 3), ("B", 1, 4), ("C", 2, 1), ("B", 2, 3), ("E", 1, 2),
    ("share", 0, 0, 1), ("A", 0, 5), ("C", 2, 0), ("E", 0, 1), ("A", 2, 4), ("B", 3, 2),
    ("A", 1, 5), ("C", 2, 2), ("C", 0, 4), ("share", 0, 0, 2), ("E", 1, 1), ("C", 0, 0),
    ("C", 1, 4), ("share", 0, 0, 3), ("prep", 0), ("E", 1, 0), ("A", 3, 2), ("A", 2, 5),
    ("A", 0, 6), ("C", 1, 3), ("B", 2, 4), ("E", 2, 2), ("A", 5, 0), ("A", 4, 2), ("E", 1, 4),
    ("A", 1, 6), ("E", 0, 3), ("E", 0, 4), ("E", 2, 1), ("E", 2, 0), ("E", 0, 2), ("E", 0, 0),
    ("C", 3, 1), ("C", 2, 3), ("E", 1, 3), ("C", 3, 0), ("ug", 0, 0), ("ug", 0, 1), ("ug", 0, 2),
    ("halo", 0, 1), ("halo", 0, 0), ("halo", 0, 2), ("B", 5, 1), ("C", 2, 4), ("B", 3, 3),
    ("A", 3, 3), ("E", 2, 3), ("B", 4, 2), ("A", 5, 1), ("conv", 0), ("down", 0, 0), ("A", 2, 6),
    ("sum", 0, 0, 0), ("sum", 0, 0, 1), ("A", 4, 3), ("E", 2, 4), ("down", 0, 1), ("B", 5, 2),
    ("sum", 0, 1, 0), ("sum", 0, 1, 1), ("E", 3, 0), ("B", 3, 4), ("B", 4, 3), ("C", 5, 1),
    ("sum", 0, 0, 2), ("A", 5, 2), ("C", 3, 3), ("sum", 0, 1, 2), ("B", 4, 4), ("A", 3, 4),
    ("scale",), ("sum", 0, 0, 3), ("C", 4, 3), ("A", 4, 4), ("C", 4, 1), ("share", 1, 0, 0),
    ("sum", 0, 1, 3), ("share", 1, 1, 0), ("C", 3, 2), ("A", 3, 5), ("B", 5, 3), ("C", 4, 0),
    ("A", 5, 3), ("share", 1, 0, 1), ("share", 1, 1, 1), ("C", 3, 4), ("C", 4, 4), ("A", 4, 5),
    ("C", 4, 2), ("E", 4, 3), ("E", 3, 1), ("E", 5, 1), ("share", 1, 0, 2), ("C", 5, 2),
    ("E", 4, 1), ("E", 3, 2), ("B", 5, 4), ("E", 3, 3), ("A", 3, 6), ("share", 1, 1, 2),
    ("E", 3, 4), ("C", 5, 3), ("share", 1, 0, 3), ("A", 5, 4), ("E", 4, 4), ("share", 1, 1, 3),
    ("prep", 1), ("A", 4, 6), ("E", 4, 0), ("E", 4, 2), ("ug", 1, 0), ("halo", 1, 0), ("ug", 1, 1),
    ("halo", 1, 1), ("ug", 1, 2), ("halo", 1, 2), ("E", 5, 3), ("E", 5, 2), ("C", 5, 0),
    ("C", 5, 4), ("A", 5, 5), ("conv", 1), ("down", 1, 3), ("sum", 1, 3, 0), ("down", 1, 2),
    ("sum", 1, 2, 0), ("down", 1, 1), ("sum", 1, 1, 0), ("sum", 1, 3, 1), ("E", 5, 0),
    ("down", 1, 0), ("sum", 1, 0, 0), ("sum", 1, 2, 1), ("sum", 1, 1, 1), ("sum", 1, 0, 1),
    ("A", 5, 6), ("sum", 1, 3, 2), ("sum", 1, 2, 2), ("E", 5, 4), ("down", 1, 4), ("sum", 1, 4, 0),
    ("sum", 1, 4, 1), ("sum", 1, 0, 2), ("sum", 1, 1, 2), ("sum", 1, 3, 3), ("sum", 1, 2, 3),
    ("sum", 1, 4, 2), ("sum", 1, 0, 3), ("sum", 1, 1, 3), ("sum", 1, 4, 3), ("out", 3),
    ("share", 2, 3, 0), ("out", 2), ("share", 2, 2, 0), ("out", 1), ("share", 2, 1, 0), ("out", 0),
    ("share", 2, 0, 0), ("share", 2, 3, 1), ("out", 4), ("share", 2, 4, 0), ("share", 2, 2, 1),
    ("share", 2, 0, 1), ("share", 2, 1, 1), ("share", 2, 4, 1), ("share", 2, 3, 2),
    ("share", 2, 3, 3), ("share", 2, 0, 2), ("share", 2, 2, 2), ("share", 2, 1, 2),
    ("share", 2, 4, 2), ("share", 2, 1, 3), ("share", 2, 0, 3), ("fin", 0), ("fin", 3),
    ("share", 2, 2, 3), ("fin", 2), ("fin", 1), ("share", 2, 4, 3), ("fin", 4),
]


class Program:
    def __init__(self, refs):
        (
            self.tok, self.wu, self.wg, self.wd, self.gain, self.us, self.gs, self.ut, self.gt,
            self.ds, self.out, self.stage, self.scales,
            self.w, self.s, self.x, self.pre, self.halo, self.hid, self.part, self.rd, self.q,
            self.rh, self.rf, self.fin_,
            self.l_sem, self.gs_sem, self.gr_sem, self.is_sem, self.ir_sem, self.ss_sem, self.sr_sem,
            self.us_sem, self.ur_sem, self.hs_sem, self.hr_sem, self.os_sem, self.or_sem,
        ) = refs
        self.zi, self.yi = lax.axis_index("z"), lax.axis_index("y")
        self.xi, self.ci = lax.axis_index("x"), lax.axis_index("c")
        self.ri = self.zi * NY + self.yi
        self.w_copies = [
            pltpu.make_async_copy((self.wu, self.wg, self.wd)[m % 3].at[m // 3], self.stage.at[m], self.l_sem.at[m])
            for m in range(6)
        ]

    def z_of(self, slot):
        return lax.rem(self.zi + offset(slot) + NZ, NZ)

    def enter(self):
        for c in self.w_copies:
            c.start()
        barrier = pltpu.get_barrier_semaphore()

        def tell(to):
            pl.semaphore_signal(barrier, inc=1, device_id=to, device_id_type=MESH)

        tell(self.step_to("c", "p"))
        tell(self.step_to("x", "p"))
        tell(self.step_to("x", "m"))
        self.each_other(lambda o: tell({"z": o // NY, "y": lax.rem(o, NY)}))
        for m in range(6):
            self.w_copies[m].wait()
            self.w[m, self.zi, self.yi] = self.stage[m].astype(jnp.bfloat16)
        pl.semaphore_wait(barrier, NR + 2)

    def gather_region(self, i, key, d, slot, recv):
        m, c0, c1, c2 = ITEMS[i]
        sign = 1 if d == "p" else -1
        hop = int(key[2])
        back = hop if recv else hop - 1
        first, second = pl.ds(c0, c1 - c0), pl.ds(c1, c2 - c1)
        z = lax.rem(self.zi - sign * back + NZ, NZ)
        y = lax.rem(self.yi - sign * back + NY, NY)
        half = pl.ds(0 if d == "p" else 32, 32)
        w = self.w.at[m]
        if key[:2] == "Ay":
            return w.at[self.zi, y, half if hop == 2 else slice(None), first]
        if key[:2] == "Az":
            if hop == 4:
                return w.at[z, pl.ds(0 if d == "p" else 2, 2), :, first]
            return w.at[z, :, :, first]
        if key[:2] == "Bz":
            return w.at[z, self.yi, half if hop == 4 else slice(None), second]
        return w.at[self.z_of(slot), y, half if hop == 2 else slice(None), second]

    def step_to(self, link, d):
        if link == "z":
            return {"z": lax.rem(self.zi + (1 if d == "p" else NZ - 1), NZ)}
        if link == "y":
            return {"y": lax.rem(self.yi + (1 if d == "p" else NY - 1), NY)}
        if link == "x":
            return {"x": lax.rem(self.xi + (1 if d == "p" else NX - 1), NX)}
        return {"c": 1 - self.ci}

    @staticmethod
    def remote(src, dst, send, recv, to):
        return pltpu.make_async_remote_copy(
            src_ref=src, dst_ref=dst, send_sem=send, recv_sem=recv, device_id=to, device_id_type=MESH
        )

    def g_copy(self, i, key, d, slot=None, recv=False):
        region = self.gather_region(i, key, d, slot, recv)
        k = KEY[key + d] if slot is None else KEY[key + d, slot]
        return self.remote(
            region, region, self.gs_sem.at[i, k], self.gr_sem.at[i, k], self.step_to(key[1], d)
        )

    def g_send(self, i, key, slots=(None,)):
        for slot in slots:
            for d in "pm":
                self.g_copy(i, key, d, slot).start()

    def g_wait(self, i, key, slots=(None,)):
        for slot in slots:
            for d in "pm":
                self.g_copy(i, key, d, slot, True).wait_recv()

    def g_forward(self, i, came, goes, slots=(None,)):
        for slot in slots:
            for d in "pm":
                self.g_copy(i, came, d, slot, True).wait_recv()
                self.g_copy(i, goes, d, slot).start()

    def A(self, i, st):
        if st == 0:
            self.g_send(i, "Ay1")
        elif st == 1:
            self.g_forward(i, "Ay1", "Ay2")
        elif st == 2:
            self.g_wait(i, "Ay2")
            self.g_send(i, "Az1")
        elif st < 6:
            self.g_forward(i, f"Az{st - 2}", f"Az{st - 1}")
        else:
            self.g_wait(i, "Az4")

    def B(self, i, st):
        if st == 0:
            self.g_send(i, "Bz1")
        elif st < 4:
            self.g_forward(i, f"Bz{st}", f"Bz{st + 1}")
        else:
            self.g_wait(i, "Bz4")
        self.g_send(i, "By1", slots_at(st))

    def C(self, i, distance):
        self.g_forward(i, "By1", "By2", slots_at(distance))

    def E(self, i, distance):
        self.g_wait(i, "By2", slots_at(distance))

    def lanes(self, own=True):
        c = self.ci if own else 1 - self.ci
        return pl.ds(pl.multiple_of(c * 256, 256), 256)

    def in_own(self):
        cols = pl.ds(pl.multiple_of(self.ri * 512 + self.ci * 256, 256), 256)
        rows = pl.ds(pl.multiple_of(self.xi * 16, 16), 16)
        return pltpu.make_async_copy(
            self.tok.at[rows, cols], self.s.at[0, self.ri, self.xi, :, self.lanes()], self.l_sem.at[6]
        )

    def in_copy(self, other, recv=False):
        cols = pl.ds(pl.multiple_of(other * 512 + self.ci * 256, 256), 256)
        rows = pl.ds(pl.multiple_of(self.xi * 16, 16), 16)
        lands = other if recv else self.ri
        return self.remote(
            self.tok.at[rows, cols],
            self.s.at[0, lands, self.xi, :, self.lanes()],
            self.is_sem.at[other],
            self.ir_sem.at[lands],
            {"z": other // NY, "y": lax.rem(other, NY)},
        )

    def each_other(self, do):
        def body(k, carry):
            do(lax.rem(self.ri + k, NR))
            return carry

        lax.fori_loop(1, NR, body, 0)

    def in_(self, st):
        if st == 0:
            self.in_own().start()
            self.each_other(lambda o: self.in_copy(o).start())
        else:
            self.in_own().wait()
            self.each_other(lambda o: self.in_copy(o, True).wait_recv())

    def share_copy(self, which, j, key, recv=False):
        lo, n = SHARE_CHUNKS[which][j]
        if key[0] == "X":
            sign = 1 if key[2] == "p" else -1
            hop = int(key[1])
            back = hop if recv else hop - 1
            x = lax.rem(self.xi - sign * back + NX, NX)
            if hop == 2:
                n = n // 2
                lo += 0 if key[2] == "p" else n
            lanes, to = self.lanes(), self.step_to("x", key[2])
        else:
            off = {"D0": 0, "D1": NX - 1, "D2": 1, "D3": 2}[key]
            x = lax.rem(self.xi + off, NX)
            lanes, to = self.lanes(not recv), self.step_to("c", "p")
        region = self.s.at[which, pl.ds(lo, n), x, :, lanes]
        k = SHARE_KEYS[key]
        return self.remote(
            region, region, self.ss_sem.at[which, j, k], self.sr_sem.at[which, j, k], to
        )

    def share(self, which, j, st):
        def start(*keys):
            for k in keys:
                self.share_copy(which, j, k).start()

        def wait(*keys):
            for k in keys:
                self.share_copy(which, j, k, True).wait_recv()

        if st == 0:
            start("X1p", "X1m", "D0")
        elif st == 1:
            wait("X1p")
            start("X2p", "D1")
            wait("X1m")
            start("X2m", "D2")
        elif st == 2:
            wait("X2p", "X2m")
            start("D3")
        else:
            wait("D0", "D1", "D2", "D3")

    def prep(self, l):
        def body(k, acc):
            block = self.s[l, pl.ds(k * 4, 4)].reshape(256, 512)
            t = block.T.astype(jnp.float32)
            z = k if l == 0 else self.z_of(k)
            cols = pl.ds(pl.multiple_of(z * 256, 256), 256)
            self.x[:, cols] = (t * self.gain[l : l + 1, cols]).astype(jnp.bfloat16)
            sq = t * t
            return acc + sq[:, :128] + sq[:, 128:]

        acc = lax.fori_loop(0, 8, body, jnp.zeros((512, 128), jnp.float32))
        mean = jnp.sum(acc, axis=1, keepdims=True) * (1.0 / 2048)
        self.inverse = lax.rsqrt(mean + EPS)

    def ug(self, l, n):
        cols = slice(n * 256, n * 256 + 256)
        for k, scale in ((0, self.us), (1, self.gs)):
            w = self.w[3 * l + k, :, :, :, cols].reshape(2048, 256)
            raw = jnp.dot(self.x[...], w, preferred_element_type=jnp.float32)
            self.pre[k, 8:520, cols] = raw * self.inverse * scale[l : l + 1, cols]

    def halo_copy(self, l, n):
        cols = pl.ds(n * 256, 256)
        wrap = jnp.where(self.yi == NY - 1, 1, 0)
        to = {"z": lax.rem(self.zi + wrap, NZ), "y": lax.rem(self.yi + 1, NY)}
        return self.remote(
            self.pre.at[:, pl.ds(512, 8), cols], self.halo.at[l, :, :, cols],
            self.hs_sem.at[l, n], self.hr_sem.at[l, n], to,
        )

    def conv(self, l):
        for n in range(3):
            self.halo_copy(l, n).wait_recv()
        first = self.ri == 0
        for n in range(6):
            cols = slice(n * 128, n * 128 + 128)
            both = []
            for k, taps in ((0, self.ut), (1, self.gt)):
                before = self.halo[l, k, :, cols]
                self.pre[k, 0:8, cols] = jnp.where(first, jnp.zeros_like(before), before)
                total = taps[0, l : l + 1, cols] * self.pre[k, 6:518, cols]
                total += taps[1, l : l + 1, cols] * self.pre[k, 7:519, cols]
                total += taps[2, l : l + 1, cols] * self.pre[k, 8:520, cols]
                both.append(total)
            up, gate = both
            self.hid[:, cols] = (gate / (1.0 + jnp.exp(-gate)) * up).astype(jnp.bfloat16)
        for n in range(3):
            self.halo_copy(l, n).wait_send()

    def scale(self):
        def body(k, carry):
            cols = pl.ds(pl.multiple_of(k * 128, 128), 128)
            for l in range(2):
                row = jnp.broadcast_to(self.ds[l : l + 1, cols], (128, 128))
                self.scales[l, pl.ds(k * 2, 2)] = row.T.reshape(2, 4, 16, 128)
            return carry

        lax.fori_loop(0, 16, body, 0)

    def down(self, l, j):
        def body(slot, carry):
            w = self.w[3 * l + 2, self.z_of(slot)].reshape(256, 768)
            part = lax.dot_general(
                w, self.hid[...], (((1,), (1,)), ((), ())), preferred_element_type=jnp.float32
            )
            self.part[l, pl.ds(slot * NY, NY)] = part.astype(jnp.bfloat16).reshape(NY, 4, 16, 512)
            return carry

        lo, n = SUM_CHUNKS[l][j]
        lax.fori_loop(lo // NY, (lo + n) // NY, body, 0)

    def sum_copy(self, l, j, key):
        lo, n = SUM_CHUNKS[l][j]
        h = n // 2
        k = SUM_KEYS[key]
        sems = (self.us_sem.at[l, j, k], self.ur_sem.at[l, j, k])
        if key == "D":
            return self.remote(
                self.part.at[l, pl.ds(lo, n), :, :, self.lanes(False)],
                self.rd.at[l, pl.ds(lo, n)], *sems, self.step_to("c", "p"),
            )
        d = key[1]
        if key[0] == "A":
            first = lo + (0 if d == "p" else h)
            return self.remote(
                self.q.at[l, pl.ds(first, h), lax.rem(self.xi + 2, NX)],
                self.rh.at[l, 0 if d == "p" else 1, pl.ds(lo // 2, h)], *sems, self.step_to("x", d),
            )
        return self.remote(
            self.q.at[l, pl.ds(lo, n), lax.rem(self.xi + (1 if d == "p" else NX - 1), NX)],
            self.rf.at[l, 0 if d == "p" else 1, pl.ds(lo, n)], *sems, self.step_to("x", d),
        )

    def sum(self, l, j, st):
        lo, n = SUM_CHUNKS[l][j]
        h = n // 2
        f32, bf16 = jnp.float32, jnp.bfloat16
        rows = pl.ds(lo, n)
        if st == 0:
            self.sum_copy(l, j, "D").start()
        elif st == 1:
            self.sum_copy(l, j, "D").wait_recv()
            mine = self.part[l, rows, :, :, self.lanes()].astype(f32)
            self.q[l, rows] = (mine + self.rd[l, rows].astype(f32)).astype(bf16)
            self.sum_copy(l, j, "Ap").start()
            self.sum_copy(l, j, "Am").start()
        elif st == 2:
            for d, key in ((1, "p"), (-1, "m")):
                self.sum_copy(l, j, "A" + key).wait_recv()
                x = lax.rem(self.xi + d + NX, NX)
                part = pl.ds(lo + (0 if key == "p" else h), h)
                came = self.rh[l, 0 if key == "p" else 1, pl.ds(lo // 2, h)].astype(f32)
                self.q[l, part, x] = (self.q[l, part, x].astype(f32) + came).astype(bf16)
                self.sum_copy(l, j, "B" + key).start()
        else:
            self.sum_copy(l, j, "Bp").wait_recv()
            self.sum_copy(l, j, "Bm").wait_recv()
            for slot in range(lo // NY, (lo + n) // NY):
                near, place = pl.ds(slot * NY, NY), pl.ds(self.z_of(slot) * NY, NY)
                total = self.q[l, near, self.xi].astype(f32)
                total += self.rf[l, 0, near].astype(f32) + self.rf[l, 1, near].astype(f32)
                scale = self.scales[l, place, self.xi]
                scale = jnp.concatenate([scale, scale], axis=2)
                old = self.s[l, place if l == 0 else near, self.xi, :, self.lanes()].astype(f32)
                new = (total * scale + RESIDUAL * old).astype(bf16)
                if l == 0:
                    self.s[1, near, self.xi, :, self.lanes()] = new
                else:
                    self.fin_[near] = new
            if l == 1:
                self.each_out(j, lambda slot, y: self.out_copy(slot, y).start())

    def out_copy(self, slot, y, recv=False):
        if recv:
            here, there = slot * NY + y, slot * NY + y
        else:
            here, there = slot * NY + y, opposite(slot) * NY + self.yi
        return self.remote(
            self.fin_.at[here],
            self.s.at[2, there, self.xi, :, self.lanes()],
            self.os_sem.at[here],
            self.or_sem.at[there],
            {"z": self.z_of(slot), "y": y},
        )

    def each_out(self, j, do):
        lo, n = SUM_CHUNKS[1][j]
        for slot in range(lo // NY, (lo + n) // NY):
            for k in range(1 if slot == 0 else 0, NY):
                do(slot, lax.rem(self.yi + k, NY))

    def out_(self, j):
        if j == 0:
            self.s[2, self.yi, self.xi, :, self.lanes()] = self.fin_[self.yi]
        self.each_out(j, lambda slot, y: self.out_copy(slot, y, True).wait_recv())

    def fin_copy(self, slot):
        return pltpu.make_async_copy(
            self.s.at[2, pl.ds(slot * NY, NY)],
            self.out.at[pl.ds(self.z_of(slot) * NY, NY)],
            self.l_sem.at[7 + slot],
        )

    def fin(self, j):
        lo, n = SHARE_CHUNKS[2][j]
        for slot in range(lo // NY, (lo + n) // NY):
            self.fin_copy(slot).start()

    def run(self):
        self.enter()
        for event in ORDER:
            name, rest = event[0], event[1:]
            if name == "halo":
                self.halo_copy(*rest).start()
            elif name in ("in", "out"):
                getattr(self, name + "_")(*rest)
            else:
                getattr(self, name)(*rest)
        for i in range(len(ITEMS)):
            for k in PAIR_KEYS:
                for d in "pm":
                    self.g_copy(i, k, d).wait_send()
            for k in ("By1", "By2"):
                for slot in range(NZ):
                    for d in "pm":
                        self.g_copy(i, k, d, slot).wait_send()
        self.each_other(lambda o: self.in_copy(o).wait_send())
        for which in range(3):
            for j in range(len(SHARE_CHUNKS[which])):
                for k in SHARE_KEYS:
                    self.share_copy(which, j, k).wait_send()
        for l in range(2):
            for j in range(len(SUM_CHUNKS[l])):
                for k in SUM_KEYS:
                    self.sum_copy(l, j, k).wait_send()
        for j in range(len(SUM_CHUNKS[1])):
            self.each_out(j, lambda slot, y: self.out_copy(slot, y).wait_send())
        for slot in range(NZ):
            self.fin_copy(slot).wait()


def kernel(*refs):
    Program(refs).run()


def per_device(
    tokens, norm_gain, up_weight, gate_weight, up_scale, gate_scale, up_taps, gate_taps,
    down_weight, down_scale,
):
    bf16, f32 = jnp.bfloat16, jnp.float32
    vmem, hbm = pl.BlockSpec(memory_space=pltpu.VMEM), pl.BlockSpec(memory_space=pl.ANY)
    dma = pltpu.SemaphoreType.DMA
    n = len(ITEMS)
    out = pl.pallas_call(
        kernel,
        out_shape=jax.ShapeDtypeStruct((NR, 4, 16, 512), bf16),
        in_specs=[hbm] * 4 + [vmem] * 6,
        out_specs=hbm,
        scratch_shapes=[
            pltpu.VMEM((6, 64, 768), f32),
            pltpu.VMEM((2, NR, 4, 16, 128), f32),
            pltpu.VMEM((6, NZ, NY, 64, 768), bf16),
            pltpu.VMEM((3, NR, 4, 16, 512), bf16),
            pltpu.VMEM((512, 2048), bf16),
            pltpu.VMEM((2, 520, 768), f32),
            pltpu.VMEM((2, 2, 8, 768), f32),
            pltpu.VMEM((512, 768), bf16),
            pltpu.VMEM((2, NR, 4, 16, 512), bf16),
            pltpu.VMEM((2, NR, 4, 16, 256), bf16),
            pltpu.VMEM((2, NR, 4, 16, 256), bf16),
            pltpu.VMEM((2, 2, NR // 2, 16, 256), bf16),
            pltpu.VMEM((2, 2, NR, 16, 256), bf16),
            pltpu.VMEM((NR, 16, 256), bf16),
            dma((15,)),
            dma((n, 52)), dma((n, 52)),
            dma((NR,)), dma((NR,)),
            dma((3, 5, 8)), dma((3, 5, 8)),
            dma((2, 5, 5)), dma((2, 5, 5)),
            dma((2, 3)), dma((2, 3)),
            dma((NR,)), dma((NR,)),
        ],
        compiler_params=pltpu.CompilerParams(
            collective_id=0, has_side_effects=True, vmem_limit_bytes=60 * 2**20
        ),
    )(
        tokens, up_weight, gate_weight, down_weight, norm_gain, up_scale, gate_scale,
        up_taps.transpose(1, 0, 2), gate_taps.transpose(1, 0, 2), down_scale,
    )
    return out.reshape(NR, 64, 512).transpose(1, 0, 2).reshape(64, NR * 512)


def solution(mesh):
    torus = Mesh(mesh.devices.reshape(NZ, NY, NX, 2), ("z", "y", "x", "c"))
    ra, cb = ("z", "y"), ("x", "c")
    placed = (
        P(ra, None),
        P(),
        P(None, ra, cb),
        P(None, ra, cb),
        P(None, cb),
        P(None, cb),
        P(None, None, cb),
        P(None, None, cb),
        P(None, ra, cb),
        P(),
    )
    return jax.shard_map(
        per_device, mesh=torus, in_specs=placed, out_specs=P(ra, None), check_vma=False
    )
```

time: 201 us -> 170 us (0.85)
  Pallas kernels: 188 us -> 166 us
  local copies, waits for them, and re-layouts: 8.53 us -> 3.11 us
  other arithmetic: 3.06 us -> 0 us
    pallas_call x1, Pallas kernels: 188 us -> 166 us  [per_device(): pl.pallas_call(kernel, out_shape=jax.ShapeDtypeStruct((NR, 4, 16, 512), b...]
    unnamed x9 -> x0, local copies, waits for them, and re-layouts: 3.51 us -> none
    another operation x3 -> x0, other arithmetic: 3.06 us -> none
where the time goes in v2:
time: 170 us
  Pallas kernels  166 us (98%)
  local copies, waits for them, and re-layouts  3.11 us (2%)
    pallas_call x1, Pallas kernels, per_device(): pl.pallas_call(kernel, out_shape=jax.ShapeDtypeStruct((NR, 4, 16, 512), b...  166 us

profile of v2, /device:TPU:1, one launch (start us, length us, event | category | flops | bytes accessed | tf_op | source)
XLA Modules:
  0.0 169.6 jit_solution(6871054021020170848)
XLA Ops:
  0.0 166.5 %shard_map.100 = bf16[32,4,16,512]{3,2,1,0:T(8,128)(2,1)} custom-call(bf16[64,16384]{1,0:T(8,128)(2,1)} %refs_0_.1, f32[2,64,768]{2,1,0:T(8,128)} %refs_1_.1, f32[2,64,768]{2,1,0:T(8,128)} %refs_2_.1, f32[2,64,768]{2,1,0:T(8,128)} %refs_3_.1, f32[2,2048]{1,0:T(2,128)} %refs_4_.1, f32[2,768]{1,0:T(2,128)} %refs_5_.1, f32[2,768]{1,0:T(2,128)} %refs_6_.1, ...), custom_call_target="tpu_custom_call" | custom-call | tf_op jit(solution)/shard_map/pallas_call | solution.py:504
  166.5 3.1 %copy.12 = bf16[32,8,8,512]{3,2,0,1:T(8,128)(2,1)} copy(bf16[32,8,8,512]{3,2,1,0:T(8,128)(2,1)} %bitcast.7) | data formatting | bytes 4194304 | tf_op jit(solution)/shard_map/reshape | solution.py:539

commit v3 on v2

v3 whole, which is shorter than its diff:
```python
import jax
import jax.numpy as jnp
from jax import lax
from jax.experimental import pallas as pl
from jax.experimental.pallas import tpu as pltpu
from jax.sharding import Mesh
from jax.sharding import PartitionSpec as P

MESH = pl.DeviceIdType.MESH
EPS = 1e-06
RESIDUAL = 0.5
NZ, NY, NX = 8, 4, 4
NR = NZ * NY

ITEMS = [(0, 0, 384, 768), (1, 0, 256, 768), (2, 0, 256, 768), (3, 0, 384, 768), (4, 0, 256, 768), (5, 0, 256, 768)]
PAIR_KEYS = ("Ay1", "Ay2", "Az1", "Az2", "Az3", "Az4", "Bz1", "Bz2", "Bz3", "Bz4")
KEY = {k: i for i, k in enumerate(PAIR_KEYS)}
for _k, _name in enumerate(("By1", "By2")):
    for _distance in range(5):
        KEY[_name, _distance] = 10 + 5 * _k + _distance

NEAR = ((0, 4), (4, 8), (12, 8), (20, 8), (28, 4))
HALVES = ((0, 16), (16, 16))
SHARE_CHUNKS = (HALVES, HALVES, NEAR)
SUM_CHUNKS = (HALVES, NEAR)
SHARE_SEMS = 3 * 9
SUM_SEMS = 3 * 7


def offset(slot):
    return (slot + 1) // 2 * (2 * (slot % 2) - 1)


def slots_at(distance):
    return (0,) if distance == 0 else (7,) if distance == 4 else (2 * distance - 1, 2 * distance)


def distance_of(slot):
    return (slot + 1) // 2


def opposite(slot):
    return slot if slot in (0, 7) else slot + 1 if slot % 2 else slot - 1


ORDER = [
    ("know", 0), ("A", 2, 0), ("know", 1), ("B", 1, 0), ("know", 2), ("B", 3, 0), ("know", 3),
    ("B", 5, 0), ("know", 4), ("B", 2, 0), ("know", 5), ("A", 0, 0), ("A", 1, 0), ("in", 0),
    ("A", 2, 1), ("A", 3, 0), ("A", 1, 1), ("B", 2, 1), ("B", 4, 0), ("A", 3, 1), ("B", 0, 0),
    ("A", 0, 1), ("A", 1, 2), ("A", 2, 2), ("B", 0, 1), ("B", 1, 1), ("in", 1), ("share", 0, 1, 0),
    ("A", 0, 2), ("B", 2, 2), ("B", 1, 2), ("B", 0, 2), ("A", 1, 3), ("C", 1, 1), ("A", 0, 3),
    ("A", 4, 0), ("B", 3, 1), ("B", 0, 3), ("C", 1, 0), ("A", 4, 1), ("C", 1, 2), ("C", 0, 1),
    ("B", 1, 3), ("share", 0, 0, 0), ("B", 4, 1), ("share", 0, 1, 1), ("A", 0, 4), ("B", 0, 4),
    ("A", 1, 4), ("A", 2, 3), ("share", 0, 1, 2), ("C", 0, 2), ("share", 0, 1, 3), ("C", 0, 3),
    ("B", 1, 4), ("C", 2, 1), ("B", 2, 3), ("E", 1, 2), ("share", 0, 0, 1), ("A", 0, 5),
    ("C", 2, 0), ("E", 0, 1), ("A", 2, 4), ("B", 3, 2), ("A", 1, 5), ("C", 2, 2), ("C", 0, 4),
    ("share", 0, 0, 2), ("E", 1, 1), ("C", 0, 0), ("C", 1, 4), ("share", 0, 0, 3), ("prep", 0),
    ("E", 1, 0), ("A", 3, 2), ("A", 2, 5), ("A", 0, 6), ("C", 1, 3), ("B", 2, 4), ("E", 2, 2),
    ("A", 5, 0), ("A", 4, 2), ("E", 1, 4), ("A", 1, 6), ("E", 0, 3), ("E", 0, 4), ("E", 2, 1),
    ("E", 2, 0), ("E", 0, 2), ("E", 0, 0), ("C", 3, 1), ("C", 2, 3), ("E", 1, 3), ("C", 3, 0),
    ("ug", 0, 0), ("ug", 0, 1), ("ug", 0, 2), ("halo", 0, 1), ("halo", 0, 0), ("halo", 0, 2),
    ("B", 5, 1), ("C", 2, 4), ("B", 3, 3), ("A", 3, 3), ("E", 2, 3), ("B", 4, 2), ("A", 5, 1),
    ("conv", 0), ("down", 0, 0), ("A", 2, 6), ("sum", 0, 0, 0), ("sum", 0, 0, 1), ("A", 4, 3),
    ("E", 2, 4), ("down", 0, 1), ("B", 5, 2), ("sum", 0, 1, 0), ("sum", 0, 1, 1), ("E", 3, 0),
    ("B", 3, 4), ("B", 4, 3), ("C", 5, 1), ("sum", 0, 0, 2), ("A", 5, 2), ("C", 3, 3),
    ("sum", 0, 1, 2), ("B", 4, 4), ("A", 3, 4), ("scale",), ("sum", 0, 0, 3), ("C", 4, 3),
    ("A", 4, 4), ("C", 4, 1), ("share", 1, 0, 0), ("sum", 0, 1, 3), ("share", 1, 1, 0), ("C", 3, 2),
    ("A", 3, 5), ("B", 5, 3), ("C", 4, 0), ("A", 5, 3), ("share", 1, 0, 1), ("share", 1, 1, 1),
    ("C", 3, 4), ("C", 4, 4), ("A", 4, 5), ("C", 4, 2), ("E", 4, 3), ("E", 3, 1), ("E", 5, 1),
    ("share", 1, 0, 2), ("C", 5, 2), ("E", 4, 1), ("E", 3, 2), ("B", 5, 4), ("E", 3, 3),
    ("A", 3, 6), ("share", 1, 1, 2), ("E", 3, 4), ("C", 5, 3), ("share", 1, 0, 3), ("A", 5, 4),
    ("E", 4, 4), ("share", 1, 1, 3), ("prep", 1), ("A", 4, 6), ("E", 4, 0), ("E", 4, 2),
    ("ug", 1, 0), ("halo", 1, 0), ("ug", 1, 1), ("halo", 1, 1), ("ug", 1, 2), ("halo", 1, 2),
    ("E", 5, 3), ("E", 5, 2), ("C", 5, 0), ("C", 5, 4), ("A", 5, 5), ("conv", 1), ("down", 1, 3),
    ("sum", 1, 3, 0), ("down", 1, 2), ("sum", 1, 2, 0), ("down", 1, 1), ("sum", 1, 1, 0),
    ("sum", 1, 3, 1), ("E", 5, 0), ("down", 1, 0), ("sum", 1, 0, 0), ("sum", 1, 2, 1),
    ("sum", 1, 1, 1), ("sum", 1, 0, 1), ("A", 5, 6), ("sum", 1, 3, 2), ("sum", 1, 2, 2),
    ("E", 5, 4), ("down", 1, 4), ("sum", 1, 4, 0), ("sum", 1, 4, 1), ("sum", 1, 0, 2),
    ("sum", 1, 1, 2), ("sum", 1, 3, 3), ("sum", 1, 2, 3), ("sum", 1, 4, 2), ("sum", 1, 0, 3),
    ("sum", 1, 1, 3), ("sum", 1, 4, 3), ("out", 3), ("share", 2, 3, 0), ("out", 2),
    ("share", 2, 2, 0), ("out", 1), ("share", 2, 1, 0), ("out", 0), ("share", 2, 0, 0),
    ("share", 2, 3, 1), ("out", 4), ("share", 2, 4, 0), ("share", 2, 2, 1), ("share", 2, 0, 1),
    ("share", 2, 1, 1), ("share", 2, 4, 1), ("share", 2, 3, 2), ("share", 2, 3, 3),
    ("share", 2, 0, 2), ("share", 2, 2, 2), ("share", 2, 1, 2), ("share", 2, 4, 2),
    ("share", 2, 1, 3), ("share", 2, 0, 3), ("fin", 0), ("fin", 3), ("share", 2, 2, 3), ("fin", 2),
    ("fin", 1), ("share", 2, 4, 3), ("fin", 4),
]


class Program:
    def __init__(self, refs):
        (
            self.tok, self.wu, self.wg, self.wd, self.gain, self.us, self.gs, self.ut, self.gt,
            self.ds, self.out, self.stage, self.scales,
            self.w, self.s, self.x, self.pre, self.halo, self.hid, self.part, self.rd, self.q,
            self.rh, self.rf, self.fin_,
            self.l_sem, self.g_send_sem, self.g_sem, self.i_send_sem, self.i_sem,
            self.s_send_sem, self.s_sem, self.u_send_sem, self.u_sem, self.h_send_sem, self.h_sem,
            self.o_send_sem, self.o_sem, self.know_sem,
        ) = refs
        self.zi, self.yi = lax.axis_index("z"), lax.axis_index("y")
        self.xi, self.ci = lax.axis_index("x"), lax.axis_index("c")
        self.ri = self.zi * NY + self.yi
        self.w_copies = [
            pltpu.make_async_copy((self.wu, self.wg, self.wd)[m % 3].at[m // 3], self.stage.at[m], self.l_sem.at[0])
            for m in range(6)
        ]

    def z_of(self, slot):
        return lax.rem(self.zi + offset(slot) + NZ, NZ)

    def enter(self):
        for c in self.w_copies:
            c.start()
        barrier = pltpu.get_barrier_semaphore()

        def tell(to):
            pl.semaphore_signal(barrier, inc=1, device_id=to, device_id_type=MESH)

        tell(self.step_to("c", "p"))
        for link in "xyz":
            for d in "pm":
                tell(self.step_to(link, d))
        pltpu.make_async_copy(self.stage, self.stage, self.l_sem.at[0]).wait()
        for m in range(6):
            self.w[m, self.ri] = self.stage[m].astype(jnp.bfloat16)
        pl.semaphore_wait(barrier, 7)

    def know(self, k):
        if k > 0:
            pl.semaphore_wait(self.know_sem.at[k - 1], 2)
        if k < 5:
            for d in "pm":
                pl.semaphore_signal(
                    self.know_sem.at[k], inc=1, device_id=self.step_to("y" if k == 0 else "z", d),
                    device_id_type=MESH,
                )

    def gather_region(self, i, key, d, slot):
        m, c0, c1, c2 = ITEMS[i]
        sign = 1 if d == "p" else -1
        hop = int(key[2])
        back = hop - 1
        first, second = pl.ds(c0, c1 - c0), pl.ds(c1, c2 - c1)
        z = lax.rem(self.zi - sign * back + NZ, NZ)
        y = lax.rem(self.yi - sign * back + NY, NY)
        half = pl.ds(0 if d == "p" else 32, 32)
        w = self.w.at[m]
        if key[:2] == "Ay":
            return w.at[self.zi * NY + y, half if hop == 2 else slice(None), first]
        if key[:2] == "Az":
            if hop == 4:
                return w.at[pl.ds(z * NY + (0 if d == "p" else 2), 2), :, first]
            return w.at[pl.ds(z * NY, NY), :, first]
        if key[:2] == "Bz":
            return w.at[z * NY + self.yi, half if hop == 4 else slice(None), second]
        return w.at[self.z_of(slot) * NY + y, half if hop == 2 else slice(None), second]

    def step_to(self, link, d):
        if link == "z":
            return {"z": lax.rem(self.zi + (1 if d == "p" else NZ - 1), NZ)}
        if link == "y":
            return {"y": lax.rem(self.yi + (1 if d == "p" else NY - 1), NY)}
        if link == "x":
            return {"x": lax.rem(self.xi + (1 if d == "p" else NX - 1), NX)}
        return {"c": 1 - self.ci}

    @staticmethod
    def remote(src, dst, send, recv, to):
        return pltpu.make_async_remote_copy(
            src_ref=src, dst_ref=dst, send_sem=send, recv_sem=recv, device_id=to, device_id_type=MESH
        )

    def g_copy(self, i, key, d, slot=None):
        region = self.gather_region(i, key, d, slot)
        k = KEY[key] if slot is None else KEY[key, distance_of(slot)]
        return self.remote(
            region, region, self.g_send_sem.at[0], self.g_sem.at[i, k], self.step_to(key[1], d)
        )

    def g_send(self, i, key, slots=(None,)):
        for slot in slots:
            for d in "pm":
                self.g_copy(i, key, d, slot).start()

    def await_bytes(self, like, sem):
        pltpu.make_async_copy(like, like, sem).wait()

    def g_wait(self, i, key, distance=None):
        m, c0, c1, c2 = ITEMS[i]
        cols = pl.ds(c0, c1 - c0) if key[0] == "A" else pl.ds(c1, c2 - c1)
        shards = {"Ay1": 2, "Ay2": 1, "Az4": 4, "Bz4": 1}.get(key, 8 if key[:2] == "Az" else 2)
        k = KEY[key] if distance is None else KEY[key, distance]
        if distance is not None:
            shards = len(slots_at(distance)) * (2 if key == "By1" else 1)
        self.await_bytes(self.w.at[m, pl.ds(0, shards), :, cols], self.g_sem.at[i, k])

    def g_forward(self, i, came, goes):
        self.g_wait(i, came)
        self.g_send(i, goes)

    def A(self, i, st):
        if st == 0:
            self.g_send(i, "Ay1")
        elif st == 1:
            self.g_forward(i, "Ay1", "Ay2")
        elif st == 2:
            self.g_wait(i, "Ay2")
            self.g_send(i, "Az1")
        elif st < 6:
            self.g_forward(i, f"Az{st - 2}", f"Az{st - 1}")
        else:
            self.g_wait(i, "Az4")

    def B(self, i, st):
        if st == 0:
            self.g_send(i, "Bz1")
        elif st < 4:
            self.g_forward(i, f"Bz{st}", f"Bz{st + 1}")
        else:
            self.g_wait(i, "Bz4")
        self.g_send(i, "By1", slots_at(st))

    def C(self, i, distance):
        self.g_wait(i, "By1", distance)
        self.g_send(i, "By2", slots_at(distance))

    def E(self, i, distance):
        self.g_wait(i, "By2", distance)

    def lanes(self, own=True):
        c = self.ci if own else 1 - self.ci
        return pl.ds(pl.multiple_of(c * 256, 256), 256)

    def rows(self, x):
        return pl.ds(pl.multiple_of(x * 16, 16), 16)

    def in_own(self):
        cols = pl.ds(pl.multiple_of(self.ri * 512 + self.ci * 256, 256), 256)
        rows = pl.ds(pl.multiple_of(self.xi * 16, 16), 16)
        return pltpu.make_async_copy(
            self.tok.at[rows, cols], self.s.at[0, self.ri, self.rows(self.xi), self.lanes()], self.l_sem.at[1]
        )

    def in_copy(self, other):
        cols = pl.ds(pl.multiple_of(other * 512 + self.ci * 256, 256), 256)
        rows = pl.ds(pl.multiple_of(self.xi * 16, 16), 16)
        return self.remote(
            self.tok.at[rows, cols],
            self.s.at[0, self.ri, self.rows(self.xi), self.lanes()],
            self.i_send_sem.at[0],
            self.i_sem.at[0],
            {"z": other // NY, "y": lax.rem(other, NY)},
        )

    def each_other(self, do):
        def body(k, carry):
            do(lax.rem(self.ri + k, NR))
            return carry

        lax.fori_loop(1, NR, body, 0)

    def in_(self, st):
        if st == 0:
            self.in_own().start()
            self.each_other(lambda o: self.in_copy(o).start())
        else:
            self.in_own().wait()
            self.await_bytes(self.fin_.at[pl.ds(0, NR - 1)], self.i_sem.at[0])

    def share_copy(self, which, j, key):
        lo, n = SHARE_CHUNKS[which][j]
        sem = self.s_sem.at[(2 * which + j) * 3 + {"X1": 0, "X2": 1}.get(key[:2], 2)]
        if key[0] == "X":
            sign = 1 if key[2] == "p" else -1
            hop = int(key[1])
            x = lax.rem(self.xi - sign * (hop - 1) + NX, NX)
            if hop == 2:
                n = n // 2
                lo += 0 if key[2] == "p" else n
            to = self.step_to("x", key[2])
        else:
            x = lax.rem(self.xi + {"D0": 0, "D1": NX - 1, "D2": 1, "D3": 2}[key], NX)
            to = self.step_to("c", "p")
        region = self.s.at[which, pl.ds(lo, n), self.rows(x), self.lanes()]
        return self.remote(region, region, self.s_send_sem.at[0], sem, to)

    def share(self, which, j, st):
        lo, n = SHARE_CHUNKS[which][j]
        sem = (2 * which + j) * 3

        def start(*keys):
            for k in keys:
                self.share_copy(which, j, k).start()

        def arrived(quarters, k):
            like = self.s.at[which, pl.ds(lo, n), pl.ds(0, 16 * quarters), self.lanes()]
            self.await_bytes(like, self.s_sem.at[sem + k])

        if st == 0:
            start("X1p", "X1m", "D0")
        elif st == 1:
            arrived(2, 0)
            start("X2p", "X2m", "D1", "D2")
        elif st == 2:
            arrived(1, 1)
            start("D3")
        else:
            arrived(4, 2)

    def prep(self, l):
        def body(k, acc):
            block = self.s[l, pl.ds(k * 4, 4)].reshape(256, 512)
            t = block.T.astype(jnp.float32)
            z = k if l == 0 else self.z_of(k)
            cols = pl.ds(pl.multiple_of(z * 256, 256), 256)
            self.x[:, cols] = (t * self.gain[l : l + 1, cols]).astype(jnp.bfloat16)
            sq = t * t
            return acc + sq[:, :128] + sq[:, 128:]

        acc = lax.fori_loop(0, 8, body, jnp.zeros((512, 128), jnp.float32))
        mean = jnp.sum(acc, axis=1, keepdims=True) * (1.0 / 2048)
        self.inverse = lax.rsqrt(mean + EPS)

    def ug(self, l, n):
        cols = slice(n * 256, n * 256 + 256)
        for k, scale in ((0, self.us), (1, self.gs)):
            w = self.w[3 * l + k, :, :, cols].reshape(2048, 256)
            raw = jnp.dot(self.x[...], w, preferred_element_type=jnp.float32)
            self.pre[k, 8:520, cols] = raw * self.inverse * scale[l : l + 1, cols]

    def halo_copy(self, l, n):
        cols = pl.ds(n * 256, 256)
        wrap = jnp.where(self.yi == NY - 1, 1, 0)
        to = {"z": lax.rem(self.zi + wrap, NZ), "y": lax.rem(self.yi + 1, NY)}
        return self.remote(
            self.pre.at[:, pl.ds(512, 8), cols], self.halo.at[l, :, :, cols],
            self.h_send_sem.at[l], self.h_sem.at[l], to,
        )

    def conv(self, l):
        self.await_bytes(self.halo.at[l], self.h_sem.at[l])
        first = self.ri == 0
        for n in range(6):
            cols = slice(n * 128, n * 128 + 128)
            both = []
            for k, taps in ((0, self.ut), (1, self.gt)):
                before = self.halo[l, k, :, cols]
                self.pre[k, 0:8, cols] = jnp.where(first, jnp.zeros_like(before), before)
                total = taps[0, l : l + 1, cols] * self.pre[k, 6:518, cols]
                total += taps[1, l : l + 1, cols] * self.pre[k, 7:519, cols]
                total += taps[2, l : l + 1, cols] * self.pre[k, 8:520, cols]
                both.append(total)
            up, gate = both
            self.hid[:, cols] = (gate / (1.0 + jnp.exp(-gate)) * up).astype(jnp.bfloat16)
        self.await_bytes(self.halo.at[l], self.h_send_sem.at[l])

    def scale(self):
        def body(k, carry):
            cols = pl.ds(pl.multiple_of(k * 128, 128), 128)
            for l in range(2):
                row = jnp.broadcast_to(self.ds[l : l + 1, cols], (128, 128))
                self.scales[l, pl.ds(k * 2, 2)] = row.T.reshape(2, 4, 16, 128)
            return carry

        lax.fori_loop(0, 16, body, 0)

    def down(self, l, j):
        def body(slot, carry):
            w = self.w[3 * l + 2, pl.ds(self.z_of(slot) * NY, NY)].reshape(256, 768)
            part = lax.dot_general(
                w, self.hid[...], (((1,), (1,)), ((), ())), preferred_element_type=jnp.float32
            )
            self.part[l, pl.ds(slot * NY, NY)] = part.astype(jnp.bfloat16).reshape(NY, 4, 16, 512)
            return carry

        lo, n = SUM_CHUNKS[l][j]
        lax.fori_loop(lo // NY, (lo + n) // NY, body, 0)

    def sum_copy(self, l, j, key):
        lo, n = SUM_CHUNKS[l][j]
        h = n // 2
        k = (2 * l + j) * 3 + "DAB".index(key[0])
        sems = (self.u_send_sem.at[0], self.u_sem.at[k])
        if key == "D":
            return self.remote(
                self.part.at[l, pl.ds(lo, n), :, :, self.lanes(False)],
                self.rd.at[l, pl.ds(lo, n)], *sems, self.step_to("c", "p"),
            )
        d = key[1]
        if key[0] == "A":
            first = lo + (0 if d == "p" else h)
            return self.remote(
                self.q.at[l, pl.ds(first, h), lax.rem(self.xi + 2, NX)],
                self.rh.at[l, 0 if d == "p" else 1, pl.ds(lo // 2, h)], *sems, self.step_to("x", d),
            )
        return self.remote(
            self.q.at[l, pl.ds(lo, n), lax.rem(self.xi + (1 if d == "p" else NX - 1), NX)],
            self.rf.at[l, 0 if d == "p" else 1, pl.ds(lo, n)], *sems, self.step_to("x", d),
        )

    def sum(self, l, j, st):
        lo, n = SUM_CHUNKS[l][j]
        h = n // 2
        f32, bf16 = jnp.float32, jnp.bfloat16
        rows = pl.ds(lo, n)
        sem = (2 * l + j) * 3
        if st == 0:
            self.sum_copy(l, j, "D").start()
        elif st == 1:
            self.await_bytes(self.rd.at[l, rows], self.u_sem.at[sem])
            mine = self.part[l, rows, :, :, self.lanes()].astype(f32)
            self.q[l, rows] = (mine + self.rd[l, rows].astype(f32)).astype(bf16)
            self.sum_copy(l, j, "Ap").start()
            self.sum_copy(l, j, "Am").start()
        elif st == 2:
            self.await_bytes(self.rh.at[l, :, pl.ds(lo // 2, h)], self.u_sem.at[sem + 1])
            for d, key in ((1, "p"), (-1, "m")):
                x = lax.rem(self.xi + d + NX, NX)
                part = pl.ds(lo + (0 if key == "p" else h), h)
                came = self.rh[l, 0 if key == "p" else 1, pl.ds(lo // 2, h)].astype(f32)
                self.q[l, part, x] = (self.q[l, part, x].astype(f32) + came).astype(bf16)
                self.sum_copy(l, j, "B" + key).start()
        else:
            self.await_bytes(self.rf.at[l, :, rows], self.u_sem.at[sem + 2])
            for slot in range(lo // NY, (lo + n) // NY):
                near, place = pl.ds(slot * NY, NY), pl.ds(self.z_of(slot) * NY, NY)
                total = self.q[l, near, self.xi].astype(f32)
                total += self.rf[l, 0, near].astype(f32) + self.rf[l, 1, near].astype(f32)
                scale = self.scales[l, place, self.xi]
                scale = jnp.concatenate([scale, scale], axis=2)
                old = self.s[l, place if l == 0 else near, self.rows(self.xi), self.lanes()].astype(f32)
                new = (total * scale + RESIDUAL * old).astype(bf16)
                if l == 0:
                    self.s[1, near, self.rows(self.xi), self.lanes()] = new
                else:
                    self.fin_[near] = new
            if l == 1:
                self.each_out(j, lambda slot, y: self.out_copy(slot, y).start())

    def out_copy(self, slot, y):
        return self.remote(
            self.fin_.at[slot * NY + y],
            self.s.at[2, opposite(slot) * NY + self.yi, self.rows(self.xi), self.lanes()],
            self.o_send_sem.at[0],
            self.o_sem.at[distance_of(slot)],
            {"z": self.z_of(slot), "y": y},
        )

    def each_out(self, j, do):
        lo, n = SUM_CHUNKS[1][j]
        for slot in range(lo // NY, (lo + n) // NY):
            for k in range(1 if slot == 0 else 0, NY):
                do(slot, lax.rem(self.yi + k, NY))

    def out_(self, j):
        n = SUM_CHUNKS[1][j][1]
        if j == 0:
            n -= 1
            self.s[2, self.yi, self.rows(self.xi), self.lanes()] = self.fin_[self.yi]
        self.await_bytes(self.fin_.at[pl.ds(0, n)], self.o_sem.at[j])

    def fin_copy(self, slot):
        return pltpu.make_async_copy(
            self.s.at[2, pl.ds(slot * NY, NY)],
            self.out.at[pl.ds(self.z_of(slot) * NY, NY)],
            self.l_sem.at[2],
        )

    def fin(self, j):
        lo, n = SHARE_CHUNKS[2][j]
        for slot in range(lo // NY, (lo + n) // NY):
            self.fin_copy(slot).start()

    def run(self):
        self.enter()
        for event in ORDER:
            name, rest = event[0], event[1:]
            if name == "halo":
                self.halo_copy(*rest).start()
            elif name in ("in", "out"):
                getattr(self, name + "_")(*rest)
            else:
                getattr(self, name)(*rest)
        self.await_bytes(self.w.at[:, pl.ds(0, NR - 1)], self.g_send_sem.at[0])
        self.await_bytes(self.fin_.at[pl.ds(0, NR - 1)], self.i_send_sem.at[0])
        self.await_bytes(self.s.at[:, pl.ds(0, 28)], self.s_send_sem.at[0])
        self.await_bytes(self.s.at[pl.ds(0, 2), pl.ds(0, 28)], self.u_send_sem.at[0])
        self.await_bytes(self.fin_.at[pl.ds(0, NR - 1)], self.o_send_sem.at[0])
        self.await_bytes(self.s.at[2], self.l_sem.at[2])


def kernel(*refs):
    Program(refs).run()


def per_device(
    tokens, norm_gain, up_weight, gate_weight, up_scale, gate_scale, up_taps, gate_taps,
    down_weight, down_scale,
):
    bf16, f32 = jnp.bfloat16, jnp.float32
    vmem, hbm = pl.BlockSpec(memory_space=pltpu.VMEM), pl.BlockSpec(memory_space=pl.ANY)
    dma = pltpu.SemaphoreType.DMA
    n = len(ITEMS)
    out = pl.pallas_call(
        kernel,
        out_shape=jax.ShapeDtypeStruct((NR, 64, 512), bf16),
        in_specs=[hbm] * 4 + [vmem] * 6,
        out_specs=hbm,
        scratch_shapes=[
            pltpu.VMEM((6, 64, 768), f32),
            pltpu.VMEM((2, NR, 4, 16, 128), f32),
            pltpu.VMEM((6, NR, 64, 768), bf16),
            pltpu.VMEM((3, NR, 64, 512), bf16),
            pltpu.VMEM((512, 2048), bf16),
            pltpu.VMEM((2, 520, 768), f32),
            pltpu.VMEM((2, 2, 8, 768), f32),
            pltpu.VMEM((512, 768), bf16),
            pltpu.VMEM((2, NR, 4, 16, 512), bf16),
            pltpu.VMEM((2, NR, 4, 16, 256), bf16),
            pltpu.VMEM((2, NR, 4, 16, 256), bf16),
            pltpu.VMEM((2, 2, NR // 2, 16, 256), bf16),
            pltpu.VMEM((2, 2, NR, 16, 256), bf16),
            pltpu.VMEM((NR, 16, 256), bf16),
            dma((3,)),
            dma((1,)), dma((n, 20)),
            dma((1,)), dma((1,)),
            dma((1,)), dma((SHARE_SEMS,)),
            dma((1,)), dma((SUM_SEMS,)),
            dma((2,)), dma((2,)),
            dma((1,)), dma((5,)),
            pltpu.SemaphoreType.REGULAR((5,)),
        ],
        compiler_params=pltpu.CompilerParams(
            collective_id=0, has_side_effects=True, vmem_limit_bytes=60 * 2**20
        ),
    )(
        tokens, up_weight, gate_weight, down_weight, norm_gain, up_scale, gate_scale,
        up_taps.transpose(1, 0, 2), gate_taps.transpose(1, 0, 2), down_scale,
    )
    return out.transpose(1, 0, 2).reshape(64, NR * 512)


def solution(mesh):
    torus = Mesh(mesh.devices.reshape(NZ, NY, NX, 2), ("z", "y", "x", "c"))
    ra, cb = ("z", "y"), ("x", "c")
    placed = (
        P(ra, None),
        P(),
        P(None, ra, cb),
        P(None, ra, cb),
        P(None, cb),
        P(None, cb),
        P(None, None, cb),
        P(None, None, cb),
        P(None, ra, cb),
        P(),
    )
    return jax.shard_map(
        per_device, mesh=torus, in_specs=placed, out_specs=P(ra, None), check_vma=False
    )
```

time: 170 us -> 162 us (0.953)
  Pallas kernels: 166 us -> 158 us
    pallas_call x1, Pallas kernels: 166 us -> 158 us  [per_device(): pl.pallas_call(kernel, out_shape=jax.ShapeDtypeStruct((NR, 64, 512), bf16...]
where the time goes in v3:
time: 162 us; the launch traced here: 161 us
  Pallas kernels  158 us (98%)
  local copies, waits for them, and re-layouts  3.11 us (2%)
    pallas_call x1, Pallas kernels, per_device(): pl.pallas_call(kernel, out_shape=jax.ShapeDtypeStruct((NR, 64, 512), bf16...  158 us

profile of v3, /device:TPU:1, one launch (start us, length us, event | category | flops | bytes accessed | tf_op | source)
XLA Modules:
  0.0 161.4 jit_solution(5192614372888109063)
XLA Ops:
  0.0 158.3 %shard_map.100 = bf16[32,64,512]{2,1,0:T(8,128)(2,1)} custom-call(bf16[64,16384]{1,0:T(8,128)(2,1)} %refs_0_.1, f32[2,64,768]{2,1,0:T(8,128)} %refs_1_.1, f32[2,64,768]{2,1,0:T(8,128)} %refs_2_.1, f32[2,64,768]{2,1,0:T(8,128)} %refs_3_.1, f32[2,2048]{1,0:T(2,128)} %refs_4_.1, f32[2,768]{1,0:T(2,128)} %refs_5_.1, f32[2,768]{1,0:T(2,128)} %refs_6_.1, ...), custom_call_target="tpu_custom_call" | custom-call | tf_op jit(solution)/shard_map/pallas_call | solution.py:505
  158.3 3.1 %copy.12 = bf16[32,8,8,512]{3,2,0,1:T(8,128)(2,1)} copy(bf16[32,8,8,512]{3,2,1,0:T(8,128)(2,1)} %bitcast.5) | data formatting | bytes 4194304 | tf_op jit(solution)/shard_map/reshape | solution.py:541

commit v4 on v3

--- a/solution.py
+++ b/solution.py
@@ -12,7 +12,7 @@
 NZ, NY, NX = 8, 4, 4
 NR = NZ * NY
 
-ITEMS = [(0, 0, 384, 768), (1, 0, 256, 768), (2, 0, 256, 768), (3, 0, 384, 768), (4, 0, 256, 768), (5, 0, 256, 768)]
+ITEMS = [(0, 0, 256, 768), (1, 0, 384, 768), (2, 0, 256, 768), (3, 0, 256, 768), (4, 0, 384, 768), (5, 0, 256, 768)]
 PAIR_KEYS = ("Ay1", "Ay2", "Az1", "Az2", "Az3", "Az4", "Bz1", "Bz2", "Bz3", "Bz4")
 KEY = {k: i for i, k in enumerate(PAIR_KEYS)}
 for _k, _name in enumerate(("By1", "By2")):
@@ -21,10 +21,11 @@
 
 NEAR = ((0, 4), (4, 8), (12, 8), (20, 8), (28, 4))
 HALVES = ((0, 16), (16, 16))
-SHARE_CHUNKS = (HALVES, HALVES, NEAR)
-SUM_CHUNKS = (HALVES, NEAR)
-SHARE_SEMS = 3 * 9
-SUM_SEMS = 3 * 7
+FIRST = ((0, 8), (8, 8), (16, 8), (24, 8))
+SHARE_CHUNKS = (HALVES, FIRST, NEAR)
+SUM_CHUNKS = (FIRST, NEAR)
+SHARE_SEMS = 3 * 13
+SUM_SEMS = 3 * 10
 
 
 def offset(slot):
@@ -44,54 +45,58 @@
 
 
 ORDER = [
-    ("know", 0), ("A", 2, 0), ("know", 1), ("B", 1, 0), ("know", 2), ("B", 3, 0), ("know", 3),
-    ("B", 5, 0), ("know", 4), ("B", 2, 0), ("know", 5), ("A", 0, 0), ("A", 1, 0), ("in", 0),
-    ("A", 2, 1), ("A", 3, 0), ("A", 1, 1), ("B", 2, 1), ("B", 4, 0), ("A", 3, 1), ("B", 0, 0),
-    ("A", 0, 1), ("A", 1, 2), ("A", 2, 2), ("B", 0, 1), ("B", 1, 1), ("in", 1), ("share", 0, 1, 0),
-    ("A", 0, 2), ("B", 2, 2), ("B", 1, 2), ("B", 0, 2), ("A", 1, 3), ("C", 1, 1), ("A", 0, 3),
-    ("A", 4, 0), ("B", 3, 1), ("B", 0, 3), ("C", 1, 0), ("A", 4, 1), ("C", 1, 2), ("C", 0, 1),
-    ("B", 1, 3), ("share", 0, 0, 0), ("B", 4, 1), ("share", 0, 1, 1), ("A", 0, 4), ("B", 0, 4),
-    ("A", 1, 4), ("A", 2, 3), ("share", 0, 1, 2), ("C", 0, 2), ("share", 0, 1, 3), ("C", 0, 3),
-    ("B", 1, 4), ("C", 2, 1), ("B", 2, 3), ("E", 1, 2), ("share", 0, 0, 1), ("A", 0, 5),
-    ("C", 2, 0), ("E", 0, 1), ("A", 2, 4), ("B", 3, 2), ("A", 1, 5), ("C", 2, 2), ("C", 0, 4),
-    ("share", 0, 0, 2), ("E", 1, 1), ("C", 0, 0), ("C", 1, 4), ("share", 0, 0, 3), ("prep", 0),
-    ("E", 1, 0), ("A", 3, 2), ("A", 2, 5), ("A", 0, 6), ("C", 1, 3), ("B", 2, 4), ("E", 2, 2),
-    ("A", 5, 0), ("A", 4, 2), ("E", 1, 4), ("A", 1, 6), ("E", 0, 3), ("E", 0, 4), ("E", 2, 1),
-    ("E", 2, 0), ("E", 0, 2), ("E", 0, 0), ("C", 3, 1), ("C", 2, 3), ("E", 1, 3), ("C", 3, 0),
-    ("ug", 0, 0), ("ug", 0, 1), ("ug", 0, 2), ("halo", 0, 1), ("halo", 0, 0), ("halo", 0, 2),
-    ("B", 5, 1), ("C", 2, 4), ("B", 3, 3), ("A", 3, 3), ("E", 2, 3), ("B", 4, 2), ("A", 5, 1),
-    ("conv", 0), ("down", 0, 0), ("A", 2, 6), ("sum", 0, 0, 0), ("sum", 0, 0, 1), ("A", 4, 3),
-    ("E", 2, 4), ("down", 0, 1), ("B", 5, 2), ("sum", 0, 1, 0), ("sum", 0, 1, 1), ("E", 3, 0),
-    ("B", 3, 4), ("B", 4, 3), ("C", 5, 1), ("sum", 0, 0, 2), ("A", 5, 2), ("C", 3, 3),
-    ("sum", 0, 1, 2), ("B", 4, 4), ("A", 3, 4), ("scale",), ("sum", 0, 0, 3), ("C", 4, 3),
-    ("A", 4, 4), ("C", 4, 1), ("share", 1, 0, 0), ("sum", 0, 1, 3), ("share", 1, 1, 0), ("C", 3, 2),
-    ("A", 3, 5), ("B", 5, 3), ("C", 4, 0), ("A", 5, 3), ("share", 1, 0, 1), ("share", 1, 1, 1),
-    ("C", 3, 4), ("C", 4, 4), ("A", 4, 5), ("C", 4, 2), ("E", 4, 3), ("E", 3, 1), ("E", 5, 1),
-    ("share", 1, 0, 2), ("C", 5, 2), ("E", 4, 1), ("E", 3, 2), ("B", 5, 4), ("E", 3, 3),
-    ("A", 3, 6), ("share", 1, 1, 2), ("E", 3, 4), ("C", 5, 3), ("share", 1, 0, 3), ("A", 5, 4),
-    ("E", 4, 4), ("share", 1, 1, 3), ("prep", 1), ("A", 4, 6), ("E", 4, 0), ("E", 4, 2),
-    ("ug", 1, 0), ("halo", 1, 0), ("ug", 1, 1), ("halo", 1, 1), ("ug", 1, 2), ("halo", 1, 2),
-    ("E", 5, 3), ("E", 5, 2), ("C", 5, 0), ("C", 5, 4), ("A", 5, 5), ("conv", 1), ("down", 1, 3),
-    ("sum", 1, 3, 0), ("down", 1, 2), ("sum", 1, 2, 0), ("down", 1, 1), ("sum", 1, 1, 0),
-    ("sum", 1, 3, 1), ("E", 5, 0), ("down", 1, 0), ("sum", 1, 0, 0), ("sum", 1, 2, 1),
-    ("sum", 1, 1, 1), ("sum", 1, 0, 1), ("A", 5, 6), ("sum", 1, 3, 2), ("sum", 1, 2, 2),
-    ("E", 5, 4), ("down", 1, 4), ("sum", 1, 4, 0), ("sum", 1, 4, 1), ("sum", 1, 0, 2),
-    ("sum", 1, 1, 2), ("sum", 1, 3, 3), ("sum", 1, 2, 3), ("sum", 1, 4, 2), ("sum", 1, 0, 3),
-    ("sum", 1, 1, 3), ("sum", 1, 4, 3), ("out", 3), ("share", 2, 3, 0), ("out", 2),
-    ("share", 2, 2, 0), ("out", 1), ("share", 2, 1, 0), ("out", 0), ("share", 2, 0, 0),
-    ("share", 2, 3, 1), ("out", 4), ("share", 2, 4, 0), ("share", 2, 2, 1), ("share", 2, 0, 1),
-    ("share", 2, 1, 1), ("share", 2, 4, 1), ("share", 2, 3, 2), ("share", 2, 3, 3),
-    ("share", 2, 0, 2), ("share", 2, 2, 2), ("share", 2, 1, 2), ("share", 2, 4, 2),
-    ("share", 2, 1, 3), ("share", 2, 0, 3), ("fin", 0), ("fin", 3), ("share", 2, 2, 3), ("fin", 2),
-    ("fin", 1), ("share", 2, 4, 3), ("fin", 4),
+    ("A", 2, 0), ("A", 0, 0), ("B", 0, 0), ("B", 1, 0), ("A", 1, 0), ("B", 4, 0), ("know", 0),
+    ("B", 0, 1), ("A", 0, 1), ("B", 2, 0), ("know", 1), ("know", 2), ("know", 3), ("B", 1, 1),
+    ("A", 4, 0), ("B", 3, 0), ("B", 0, 2), ("know", 4), ("A", 1, 1), ("know", 5), ("B", 1, 2),
+    ("in", 0), ("B", 1, 3), ("A", 2, 1), ("B", 2, 1), ("A", 0, 2), ("A", 1, 2), ("in", 1),
+    ("B", 0, 3), ("A", 0, 3), ("share", 0, 0, 0), ("A", 1, 3), ("C", 1, 3), ("B", 0, 4),
+    ("C", 0, 0), ("B", 1, 4), ("A", 0, 4), ("A", 3, 0), ("C", 1, 1), ("share", 0, 1, 0),
+    ("B", 4, 1), ("B", 3, 1), ("A", 1, 4), ("C", 0, 4), ("scale",), ("C", 2, 0), ("C", 0, 2),
+    ("C", 1, 2), ("A", 3, 1), ("C", 1, 4), ("C", 0, 3), ("A", 2, 2), ("share", 0, 1, 1),
+    ("A", 1, 5), ("C", 1, 0), ("E", 2, 0), ("E", 0, 2), ("B", 2, 2), ("C", 0, 1), ("A", 4, 1),
+    ("A", 0, 5), ("E", 0, 3), ("A", 2, 3), ("B", 2, 3), ("B", 3, 2), ("E", 1, 1),
+    ("share", 0, 1, 2), ("share", 0, 1, 3), ("A", 3, 2), ("share", 0, 0, 1), ("E", 1, 0),
+    ("E", 1, 4), ("B", 5, 0), ("A", 0, 6), ("share", 0, 0, 2), ("share", 0, 0, 3), ("C", 2, 3),
+    ("A", 2, 4), ("E", 1, 2), ("E", 0, 4), ("E", 0, 0), ("E", 1, 3), ("B", 3, 3), ("prep", 0),
+    ("A", 4, 2), ("A", 1, 6), ("E", 0, 1), ("ug", 0, 0), ("ug", 0, 1), ("halo", 0, 1), ("ug", 0, 2),
+    ("halo", 0, 2), ("halo", 0, 0), ("C", 2, 2), ("C", 2, 1), ("B", 2, 4), ("B", 4, 2), ("conv", 0),
+    ("E", 2, 2), ("A", 2, 5), ("E", 2, 3), ("down", 0, 2), ("sum", 0, 2, 0), ("A", 4, 3),
+    ("A", 5, 0), ("A", 3, 3), ("E", 2, 1), ("down", 0, 0), ("sum", 0, 0, 0), ("B", 4, 3),
+    ("C", 4, 0), ("down", 0, 1), ("sum", 0, 1, 0), ("sum", 0, 2, 1), ("C", 2, 4), ("sum", 0, 0, 1),
+    ("B", 3, 4), ("A", 2, 6), ("C", 3, 1), ("A", 5, 1), ("C", 3, 2), ("sum", 0, 1, 1),
+    ("sum", 0, 2, 2), ("B", 5, 1), ("C", 3, 0), ("sum", 0, 0, 2), ("E", 4, 0), ("E", 2, 4),
+    ("down", 0, 3), ("sum", 0, 3, 0), ("sum", 0, 1, 2), ("A", 3, 4), ("C", 4, 3), ("sum", 0, 3, 1),
+    ("sum", 0, 0, 3), ("A", 4, 4), ("A", 5, 2), ("share", 1, 0, 0), ("C", 3, 4), ("sum", 0, 2, 3),
+    ("share", 1, 2, 0), ("sum", 0, 3, 2), ("B", 4, 4), ("B", 5, 2), ("share", 1, 0, 1), ("C", 4, 1),
+    ("sum", 0, 1, 3), ("C", 4, 2), ("share", 1, 1, 0), ("sum", 0, 3, 3), ("share", 1, 3, 0),
+    ("E", 3, 0), ("share", 1, 0, 2), ("share", 1, 1, 1), ("share", 1, 0, 3), ("E", 3, 4),
+    ("C", 4, 4), ("E", 3, 1), ("C", 3, 3), ("share", 1, 2, 1), ("A", 3, 5), ("share", 1, 3, 1),
+    ("A", 4, 5), ("C", 5, 2), ("E", 4, 3), ("C", 5, 0), ("A", 5, 3), ("share", 1, 2, 2),
+    ("share", 1, 1, 2), ("B", 5, 3), ("share", 1, 3, 2), ("C", 5, 1), ("E", 4, 2), ("E", 3, 2),
+    ("share", 1, 1, 3), ("share", 1, 2, 3), ("A", 3, 6), ("E", 4, 1), ("E", 4, 4),
+    ("share", 1, 3, 3), ("prep", 1), ("E", 3, 3), ("A", 4, 6), ("ug", 1, 0), ("halo", 1, 0),
+    ("ug", 1, 1), ("halo", 1, 1), ("ug", 1, 2), ("halo", 1, 2), ("A", 5, 4), ("B", 5, 4),
+    ("C", 5, 3), ("E", 5, 1), ("E", 5, 0), ("conv", 1), ("down", 1, 0), ("sum", 1, 0, 0),
+    ("down", 1, 1), ("sum", 1, 1, 0), ("E", 5, 2), ("E", 5, 3), ("A", 5, 5), ("down", 1, 3),
+    ("sum", 1, 3, 0), ("C", 5, 4), ("sum", 1, 0, 1), ("sum", 1, 1, 1), ("down", 1, 2),
+    ("sum", 1, 3, 1), ("sum", 1, 2, 0), ("E", 5, 4), ("sum", 1, 0, 2), ("sum", 1, 2, 1),
+    ("A", 5, 6), ("down", 1, 4), ("sum", 1, 4, 0), ("sum", 1, 3, 2), ("sum", 1, 0, 3),
+    ("sum", 1, 4, 1), ("sum", 1, 2, 2), ("sum", 1, 1, 2), ("sum", 1, 3, 3), ("sum", 1, 4, 2),
+    ("sum", 1, 2, 3), ("sum", 1, 1, 3), ("sum", 1, 4, 3), ("out", 0), ("share", 2, 0, 0),
+    ("out", 3), ("share", 2, 3, 0), ("out", 2), ("share", 2, 2, 0), ("share", 2, 0, 1), ("out", 1),
+    ("share", 2, 1, 0), ("share", 2, 3, 1), ("out", 4), ("share", 2, 4, 0), ("share", 2, 1, 1),
+    ("share", 2, 2, 1), ("share", 2, 0, 2), ("share", 2, 4, 1), ("share", 2, 3, 2),
+    ("share", 2, 3, 3), ("share", 2, 1, 2), ("share", 2, 0, 3), ("share", 2, 2, 2),
+    ("share", 2, 4, 2), ("fin", 0), ("share", 2, 1, 3), ("share", 2, 2, 3), ("fin", 3), ("fin", 1),
+    ("fin", 2), ("share", 2, 4, 3), ("fin", 4),
 ]
 
 
 class Program:
     def __init__(self, refs):
         (
-            self.tok, self.wu, self.wg, self.wd, self.gain, self.us, self.gs, self.ut, self.gt,
-            self.ds, self.out, self.stage, self.scales,
+            self.tok, self.wu, self.wg, self.wd, *small, self.out,
+            self.gain, self.us, self.gs, self.ut, self.gt, self.ds, self.stage, self.scales,
             self.w, self.s, self.x, self.pre, self.halo, self.hid, self.part, self.rd, self.q,
             self.rh, self.rf, self.fin_,
             self.l_sem, self.g_send_sem, self.g_sem, self.i_send_sem, self.i_sem,
@@ -106,11 +111,18 @@
             for m in range(6)
         ]
 
+        self.small_copies = [
+            pltpu.make_async_copy(a, b, self.l_sem.at[2 + k])
+            for k, (a, b) in enumerate(
+                zip(small, (self.gain, self.us, self.gs, self.ut, self.gt, self.ds), strict=True)
+            )
+        ]
+
     def z_of(self, slot):
         return lax.rem(self.zi + offset(slot) + NZ, NZ)
 
     def enter(self):
-        for c in self.w_copies:
+        for c in self.w_copies + self.small_copies:
             c.start()
         barrier = pltpu.get_barrier_semaphore()
 
@@ -270,7 +282,7 @@
 
     def share_copy(self, which, j, key):
         lo, n = SHARE_CHUNKS[which][j]
-        sem = self.s_sem.at[(2 * which + j) * 3 + {"X1": 0, "X2": 1}.get(key[:2], 2)]
+        sem = self.s_sem.at[(4 * which + j) * 3 + {"X1": 0, "X2": 1}.get(key[:2], 2)]
         if key[0] == "X":
             sign = 1 if key[2] == "p" else -1
             hop = int(key[1])
@@ -287,7 +299,7 @@
 
     def share(self, which, j, st):
         lo, n = SHARE_CHUNKS[which][j]
-        sem = (2 * which + j) * 3
+        sem = (4 * which + j) * 3
 
         def start(*keys):
             for k in keys:
@@ -366,21 +378,29 @@
         lax.fori_loop(0, 16, body, 0)
 
     def down(self, l, j):
-        def body(slot, carry):
-            w = self.w[3 * l + 2, pl.ds(self.z_of(slot) * NY, NY)].reshape(256, 768)
+        lo, n = SUM_CHUNKS[l][j]
+        width = 2 if n > NY else 1
+
+        def body(k, carry):
+            slot = lo // NY + width * k
+            w = jnp.concatenate(
+                [
+                    self.w[3 * l + 2, pl.ds(self.z_of(slot + i) * NY, NY)].reshape(256, 768)
+                    for i in range(width)
+                ]
+            )
             part = lax.dot_general(
                 w, self.hid[...], (((1,), (1,)), ((), ())), preferred_element_type=jnp.float32
-            )
-            self.part[l, pl.ds(slot * NY, NY)] = part.astype(jnp.bfloat16).reshape(NY, 4, 16, 512)
+            ).astype(jnp.bfloat16)
+            self.part[l, pl.ds(slot * NY, NY * width)] = part.reshape(NY * width, 4, 16, 512)
             return carry
 
-        lo, n = SUM_CHUNKS[l][j]
-        lax.fori_loop(lo // NY, (lo + n) // NY, body, 0)
+        lax.fori_loop(0, n // (NY * width), body, 0)
 
     def sum_copy(self, l, j, key):
         lo, n = SUM_CHUNKS[l][j]
         h = n // 2
-        k = (2 * l + j) * 3 + "DAB".index(key[0])
+        k = (4 * l + j) * 3 + "DAB".index(key[0])
         sems = (self.u_send_sem.at[0], self.u_sem.at[k])
         if key == "D":
             return self.remote(
@@ -404,7 +424,7 @@
         h = n // 2
         f32, bf16 = jnp.float32, jnp.bfloat16
         rows = pl.ds(lo, n)
-        sem = (2 * l + j) * 3
+        sem = (4 * l + j) * 3
         if st == 0:
             self.sum_copy(l, j, "D").start()
         elif st == 1:
@@ -460,22 +480,19 @@
             self.s[2, self.yi, self.rows(self.xi), self.lanes()] = self.fin_[self.yi]
         self.await_bytes(self.fin_.at[pl.ds(0, n)], self.o_sem.at[j])
 
-    def fin_copy(self, slot):
-        return pltpu.make_async_copy(
-            self.s.at[2, pl.ds(slot * NY, NY)],
-            self.out.at[pl.ds(self.z_of(slot) * NY, NY)],
-            self.l_sem.at[2],
-        )
-
     def fin(self, j):
         lo, n = SHARE_CHUNKS[2][j]
         for slot in range(lo // NY, (lo + n) // NY):
-            self.fin_copy(slot).start()
+            self.out[pl.ds(self.z_of(slot) * NY, NY)] = self.s[2, pl.ds(slot * NY, NY)]
 
     def run(self):
         self.enter()
         for event in ORDER:
             name, rest = event[0], event[1:]
+            if self.small_copies and name in ("scale", "prep"):
+                for c in self.small_copies:
+                    c.wait()
+                self.small_copies = []
             if name == "halo":
                 self.halo_copy(*rest).start()
             elif name in ("in", "out"):
@@ -487,7 +504,6 @@
         self.await_bytes(self.s.at[:, pl.ds(0, 28)], self.s_send_sem.at[0])
         self.await_bytes(self.s.at[pl.ds(0, 2), pl.ds(0, 28)], self.u_send_sem.at[0])
         self.await_bytes(self.fin_.at[pl.ds(0, NR - 1)], self.o_send_sem.at[0])
-        self.await_bytes(self.s.at[2], self.l_sem.at[2])
 
 
 def kernel(*refs):
@@ -499,15 +515,26 @@
     down_weight, down_scale,
 ):
     bf16, f32 = jnp.bfloat16, jnp.float32
-    vmem, hbm = pl.BlockSpec(memory_space=pltpu.VMEM), pl.BlockSpec(memory_space=pl.ANY)
+    hbm = pl.BlockSpec(memory_space=pltpu.HBM)
     dma = pltpu.SemaphoreType.DMA
     n = len(ITEMS)
+    arrays = (
+        tokens, up_weight, gate_weight, down_weight, norm_gain, up_scale, gate_scale,
+        up_taps.transpose(1, 0, 2), gate_taps.transpose(1, 0, 2), down_scale,
+    )
+    arrays = [pltpu.with_memory_space_constraint(a, pltpu.HBM) for a in arrays]
     out = pl.pallas_call(
         kernel,
         out_shape=jax.ShapeDtypeStruct((NR, 64, 512), bf16),
-        in_specs=[hbm] * 4 + [vmem] * 6,
-        out_specs=hbm,
+        in_specs=[hbm] * 10,
+        out_specs=pl.BlockSpec(memory_space=pltpu.VMEM),
         scratch_shapes=[
+            pltpu.VMEM((2, 2048), f32),
+            pltpu.VMEM((2, 768), f32),
+            pltpu.VMEM((2, 768), f32),
+            pltpu.VMEM((3, 2, 768), f32),
+            pltpu.VMEM((3, 2, 768), f32),
+            pltpu.VMEM((2, 2048), f32),
             pltpu.VMEM((6, 64, 768), f32),
             pltpu.VMEM((2, NR, 4, 16, 128), f32),
             pltpu.VMEM((6, NR, 64, 768), bf16),
@@ -522,7 +549,7 @@
             pltpu.VMEM((2, 2, NR // 2, 16, 256), bf16),
             pltpu.VMEM((2, 2, NR, 16, 256), bf16),
             pltpu.VMEM((NR, 16, 256), bf16),
-            dma((3,)),
+            dma((8,)),
             dma((1,)), dma((n, 20)),
             dma((1,)), dma((1,)),
             dma((1,)), dma((SHARE_SEMS,)),
@@ -532,12 +559,9 @@
             pltpu.SemaphoreType.REGULAR((5,)),
         ],
         compiler_params=pltpu.CompilerParams(
-            collective_id=0, has_side_effects=True, vmem_limit_bytes=60 * 2**20
+            collective_id=0, has_side_effects=True, vmem_limit_bytes=50 * 2**20
         ),
-    )(
-        tokens, up_weight, gate_weight, down_weight, norm_gain, up_scale, gate_scale,
-        up_taps.transpose(1, 0, 2), gate_taps.transpose(1, 0, 2), down_scale,
-    )
+    )(*arrays)
     return out.transpose(1, 0, 2).reshape(64, NR * 512)
 
 

time: 162 us -> 156 us (0.963)
  Pallas kernels: 158 us -> 154 us
    pallas_call x1, Pallas kernels: 158 us -> 154 us  [per_device(): pl.pallas_call(kernel, out_shape=jax.ShapeDtypeStruct((NR, 64, 512), bf16...]
where the time goes in v4:
time: 156 us
  Pallas kernels  154 us (99%)
    pallas_call x1, Pallas kernels, per_device(): pl.pallas_call(kernel, out_shape=jax.ShapeDtypeStruct((NR, 64, 512), bf16...  154 us

profile of v4, /device:TPU:1, one launch (start us, length us, event | category | flops | bytes accessed | tf_op | source)
XLA Modules:
  0.0 155.6 jit_solution(13085594581034196751)
XLA Ops:
  0.0 154.0 %shard_map.100 = bf16[32,64,512]{2,1,0:T(8,128)(2,1)S(1)} custom-call(bf16[64,16384]{1,0:T(8,128)(2,1)} %refs_0_.1, f32[2,64,768]{2,1,0:T(8,128)} %refs_1_.1, f32[2,64,768]{2,1,0:T(8,128)} %refs_2_.1, f32[2,64,768]{2,1,0:T(8,128)} %refs_3_.1, f32[2,2048]{1,0:T(2,128)} %refs_4_.1, f32[2,768]{1,0:T(2,128)} %refs_5_.1, f32[2,768]{1,0:T(2,128)} %refs_6_.1, ...), custom_call_target="tpu_custom_call" | custom-call | tf_op jit(solution)/shard_map/pallas_call | solution.py:526
  154.0 1.5 copy.12

commit v5 on v4

--- a/solution.py
+++ b/solution.py
@@ -45,50 +45,49 @@
 
 
 ORDER = [
-    ("A", 2, 0), ("A", 0, 0), ("B", 0, 0), ("B", 1, 0), ("A", 1, 0), ("B", 4, 0), ("know", 0),
-    ("B", 0, 1), ("A", 0, 1), ("B", 2, 0), ("know", 1), ("know", 2), ("know", 3), ("B", 1, 1),
-    ("A", 4, 0), ("B", 3, 0), ("B", 0, 2), ("know", 4), ("A", 1, 1), ("know", 5), ("B", 1, 2),
-    ("in", 0), ("B", 1, 3), ("A", 2, 1), ("B", 2, 1), ("A", 0, 2), ("A", 1, 2), ("in", 1),
-    ("B", 0, 3), ("A", 0, 3), ("share", 0, 0, 0), ("A", 1, 3), ("C", 1, 3), ("B", 0, 4),
-    ("C", 0, 0), ("B", 1, 4), ("A", 0, 4), ("A", 3, 0), ("C", 1, 1), ("share", 0, 1, 0),
-    ("B", 4, 1), ("B", 3, 1), ("A", 1, 4), ("C", 0, 4), ("scale",), ("C", 2, 0), ("C", 0, 2),
-    ("C", 1, 2), ("A", 3, 1), ("C", 1, 4), ("C", 0, 3), ("A", 2, 2), ("share", 0, 1, 1),
-    ("A", 1, 5), ("C", 1, 0), ("E", 2, 0), ("E", 0, 2), ("B", 2, 2), ("C", 0, 1), ("A", 4, 1),
-    ("A", 0, 5), ("E", 0, 3), ("A", 2, 3), ("B", 2, 3), ("B", 3, 2), ("E", 1, 1),
-    ("share", 0, 1, 2), ("share", 0, 1, 3), ("A", 3, 2), ("share", 0, 0, 1), ("E", 1, 0),
-    ("E", 1, 4), ("B", 5, 0), ("A", 0, 6), ("share", 0, 0, 2), ("share", 0, 0, 3), ("C", 2, 3),
-    ("A", 2, 4), ("E", 1, 2), ("E", 0, 4), ("E", 0, 0), ("E", 1, 3), ("B", 3, 3), ("prep", 0),
-    ("A", 4, 2), ("A", 1, 6), ("E", 0, 1), ("ug", 0, 0), ("ug", 0, 1), ("halo", 0, 1), ("ug", 0, 2),
-    ("halo", 0, 2), ("halo", 0, 0), ("C", 2, 2), ("C", 2, 1), ("B", 2, 4), ("B", 4, 2), ("conv", 0),
-    ("E", 2, 2), ("A", 2, 5), ("E", 2, 3), ("down", 0, 2), ("sum", 0, 2, 0), ("A", 4, 3),
-    ("A", 5, 0), ("A", 3, 3), ("E", 2, 1), ("down", 0, 0), ("sum", 0, 0, 0), ("B", 4, 3),
-    ("C", 4, 0), ("down", 0, 1), ("sum", 0, 1, 0), ("sum", 0, 2, 1), ("C", 2, 4), ("sum", 0, 0, 1),
-    ("B", 3, 4), ("A", 2, 6), ("C", 3, 1), ("A", 5, 1), ("C", 3, 2), ("sum", 0, 1, 1),
-    ("sum", 0, 2, 2), ("B", 5, 1), ("C", 3, 0), ("sum", 0, 0, 2), ("E", 4, 0), ("E", 2, 4),
-    ("down", 0, 3), ("sum", 0, 3, 0), ("sum", 0, 1, 2), ("A", 3, 4), ("C", 4, 3), ("sum", 0, 3, 1),
-    ("sum", 0, 0, 3), ("A", 4, 4), ("A", 5, 2), ("share", 1, 0, 0), ("C", 3, 4), ("sum", 0, 2, 3),
-    ("share", 1, 2, 0), ("sum", 0, 3, 2), ("B", 4, 4), ("B", 5, 2), ("share", 1, 0, 1), ("C", 4, 1),
-    ("sum", 0, 1, 3), ("C", 4, 2), ("share", 1, 1, 0), ("sum", 0, 3, 3), ("share", 1, 3, 0),
-    ("E", 3, 0), ("share", 1, 0, 2), ("share", 1, 1, 1), ("share", 1, 0, 3), ("E", 3, 4),
-    ("C", 4, 4), ("E", 3, 1), ("C", 3, 3), ("share", 1, 2, 1), ("A", 3, 5), ("share", 1, 3, 1),
-    ("A", 4, 5), ("C", 5, 2), ("E", 4, 3), ("C", 5, 0), ("A", 5, 3), ("share", 1, 2, 2),
-    ("share", 1, 1, 2), ("B", 5, 3), ("share", 1, 3, 2), ("C", 5, 1), ("E", 4, 2), ("E", 3, 2),
-    ("share", 1, 1, 3), ("share", 1, 2, 3), ("A", 3, 6), ("E", 4, 1), ("E", 4, 4),
-    ("share", 1, 3, 3), ("prep", 1), ("E", 3, 3), ("A", 4, 6), ("ug", 1, 0), ("halo", 1, 0),
-    ("ug", 1, 1), ("halo", 1, 1), ("ug", 1, 2), ("halo", 1, 2), ("A", 5, 4), ("B", 5, 4),
-    ("C", 5, 3), ("E", 5, 1), ("E", 5, 0), ("conv", 1), ("down", 1, 0), ("sum", 1, 0, 0),
-    ("down", 1, 1), ("sum", 1, 1, 0), ("E", 5, 2), ("E", 5, 3), ("A", 5, 5), ("down", 1, 3),
-    ("sum", 1, 3, 0), ("C", 5, 4), ("sum", 1, 0, 1), ("sum", 1, 1, 1), ("down", 1, 2),
-    ("sum", 1, 3, 1), ("sum", 1, 2, 0), ("E", 5, 4), ("sum", 1, 0, 2), ("sum", 1, 2, 1),
-    ("A", 5, 6), ("down", 1, 4), ("sum", 1, 4, 0), ("sum", 1, 3, 2), ("sum", 1, 0, 3),
-    ("sum", 1, 4, 1), ("sum", 1, 2, 2), ("sum", 1, 1, 2), ("sum", 1, 3, 3), ("sum", 1, 4, 2),
-    ("sum", 1, 2, 3), ("sum", 1, 1, 3), ("sum", 1, 4, 3), ("out", 0), ("share", 2, 0, 0),
-    ("out", 3), ("share", 2, 3, 0), ("out", 2), ("share", 2, 2, 0), ("share", 2, 0, 1), ("out", 1),
-    ("share", 2, 1, 0), ("share", 2, 3, 1), ("out", 4), ("share", 2, 4, 0), ("share", 2, 1, 1),
-    ("share", 2, 2, 1), ("share", 2, 0, 2), ("share", 2, 4, 1), ("share", 2, 3, 2),
-    ("share", 2, 3, 3), ("share", 2, 1, 2), ("share", 2, 0, 3), ("share", 2, 2, 2),
-    ("share", 2, 4, 2), ("fin", 0), ("share", 2, 1, 3), ("share", 2, 2, 3), ("fin", 3), ("fin", 1),
-    ("fin", 2), ("share", 2, 4, 3), ("fin", 4),
+    ("A", 2, 0), ("B", 1, 0), ("A", 0, 0), ("B", 2, 0), ("B", 0, 0), ("A", 2, 1), ("B", 4, 0),
+    ("B", 1, 1), ("know", 0), ("A", 1, 0), ("A", 0, 1), ("B", 2, 1), ("know", 1), ("A", 5, 0),
+    ("B", 0, 1), ("know", 2), ("A", 2, 2), ("know", 3), ("B", 1, 2), ("A", 0, 2), ("A", 1, 1),
+    ("A", 3, 0), ("know", 4), ("B", 2, 2), ("B", 0, 2), ("B", 4, 1), ("know", 5), ("A", 4, 0),
+    ("C", 0, 0), ("in", 0), ("A", 1, 2), ("B", 0, 3), ("A", 0, 3), ("A", 2, 3), ("A", 5, 1),
+    ("C", 2, 1), ("B", 2, 3), ("C", 0, 2), ("in", 1), ("B", 1, 3), ("share", 0, 0, 0), ("A", 1, 3),
+    ("A", 0, 4), ("B", 1, 4), ("C", 0, 3), ("B", 4, 2), ("A", 2, 4), ("A", 1, 4),
+    ("share", 0, 0, 1), ("A", 3, 1), ("C", 4, 0), ("share", 0, 1, 0), ("C", 1, 1), ("B", 3, 0),
+    ("C", 1, 3), ("scale",), ("B", 0, 4), ("A", 0, 5), ("share", 0, 1, 1), ("share", 0, 0, 2),
+    ("E", 0, 3), ("E", 2, 1), ("C", 0, 1), ("A", 1, 5), ("A", 2, 5), ("share", 0, 0, 3),
+    ("E", 4, 0), ("B", 4, 3), ("C", 0, 4), ("share", 0, 1, 2), ("A", 3, 2), ("E", 0, 0),
+    ("C", 1, 0), ("C", 1, 2), ("share", 0, 1, 3), ("prep", 0), ("C", 1, 4), ("B", 5, 0),
+    ("B", 3, 1), ("E", 0, 2), ("C", 2, 2), ("E", 0, 1), ("B", 2, 4), ("C", 4, 3), ("A", 4, 1),
+    ("E", 1, 3), ("A", 1, 6), ("E", 1, 1), ("A", 5, 2), ("E", 1, 2), ("E", 1, 0), ("E", 0, 4),
+    ("E", 1, 4), ("A", 0, 6), ("ug", 0, 0), ("halo", 0, 0), ("ug", 0, 1), ("A", 3, 3), ("C", 2, 0),
+    ("halo", 0, 1), ("ug", 0, 2), ("A", 2, 6), ("halo", 0, 2), ("C", 2, 3), ("C", 2, 4),
+    ("B", 3, 2), ("A", 4, 2), ("C", 4, 1), ("B", 5, 1), ("conv", 0), ("E", 2, 3), ("B", 3, 3),
+    ("E", 2, 4), ("down", 0, 3), ("sum", 0, 3, 0), ("E", 2, 2), ("down", 0, 1), ("down", 0, 2),
+    ("sum", 0, 2, 0), ("sum", 0, 1, 0), ("sum", 0, 3, 1), ("E", 2, 0), ("down", 0, 0),
+    ("sum", 0, 0, 0), ("A", 4, 3), ("sum", 0, 2, 1), ("sum", 0, 1, 1), ("C", 3, 1), ("E", 4, 3),
+    ("A", 3, 4), ("sum", 0, 0, 1), ("B", 5, 2), ("sum", 0, 3, 2), ("sum", 0, 2, 2), ("B", 3, 4),
+    ("C", 5, 1), ("sum", 0, 1, 2), ("sum", 0, 0, 2), ("sum", 0, 2, 3), ("share", 1, 2, 0),
+    ("B", 4, 4), ("A", 4, 4), ("sum", 0, 1, 3), ("share", 1, 1, 0), ("C", 3, 3), ("C", 3, 0),
+    ("sum", 0, 0, 3), ("share", 1, 0, 0), ("A", 3, 5), ("C", 5, 0), ("E", 5, 1), ("sum", 0, 3, 3),
+    ("share", 1, 3, 0), ("C", 3, 4), ("share", 1, 2, 1), ("A", 5, 3), ("C", 3, 2), ("C", 4, 4),
+    ("share", 1, 1, 1), ("C", 4, 2), ("B", 5, 3), ("share", 1, 0, 1), ("share", 1, 3, 1),
+    ("share", 1, 2, 2), ("E", 3, 4), ("share", 1, 1, 2), ("A", 4, 5), ("E", 4, 1),
+    ("share", 1, 0, 2), ("E", 3, 0), ("share", 1, 2, 3), ("E", 3, 1), ("share", 1, 3, 2),
+    ("A", 3, 6), ("C", 5, 2), ("share", 1, 1, 3), ("E", 3, 2), ("A", 5, 4), ("E", 5, 0),
+    ("E", 4, 2), ("share", 1, 0, 3), ("E", 3, 3), ("B", 5, 4), ("E", 4, 4), ("share", 1, 3, 3),
+    ("prep", 1), ("A", 4, 6), ("ug", 1, 0), ("ug", 1, 1), ("halo", 1, 1), ("halo", 1, 0),
+    ("ug", 1, 2), ("halo", 1, 2), ("E", 5, 2), ("C", 5, 4), ("A", 5, 5), ("C", 5, 3), ("conv", 1),
+    ("down", 1, 1), ("sum", 1, 1, 0), ("E", 5, 3), ("down", 1, 3), ("sum", 1, 3, 0), ("down", 1, 2),
+    ("sum", 1, 1, 1), ("sum", 1, 2, 0), ("down", 1, 0), ("sum", 1, 0, 0), ("sum", 1, 3, 1),
+    ("A", 5, 6), ("sum", 1, 2, 1), ("sum", 1, 0, 1), ("sum", 1, 1, 2), ("E", 5, 4), ("down", 1, 4),
+    ("sum", 1, 4, 0), ("sum", 1, 3, 2), ("sum", 1, 4, 1), ("sum", 1, 0, 2), ("sum", 1, 2, 2),
+    ("sum", 1, 1, 3), ("sum", 1, 3, 3), ("sum", 1, 4, 2), ("sum", 1, 0, 3), ("sum", 1, 2, 3),
+    ("sum", 1, 4, 3), ("out", 1), ("share", 2, 1, 0), ("out", 0), ("share", 2, 0, 0), ("out", 3),
+    ("share", 2, 3, 0), ("out", 2), ("share", 2, 2, 0), ("share", 2, 0, 1), ("out", 4),
+    ("share", 2, 4, 0), ("share", 2, 3, 1), ("share", 2, 1, 1), ("share", 2, 2, 1),
+    ("share", 2, 0, 2), ("share", 2, 0, 3), ("fin", 0), ("share", 2, 4, 1), ("share", 2, 3, 2),
+    ("share", 2, 1, 2), ("share", 2, 2, 2), ("share", 2, 3, 3), ("fin", 3), ("share", 2, 4, 2),
+    ("share", 2, 1, 3), ("fin", 1), ("share", 2, 2, 3), ("fin", 2), ("share", 2, 4, 3), ("fin", 4),
 ]
 
 

time: 156 us -> 153 us (0.981)
  Pallas kernels: 154 us -> 152 us
    pallas_call x1, Pallas kernels: 154 us -> 152 us  [per_device(): pl.pallas_call(kernel, out_shape=jax.ShapeDtypeStruct((NR, 64, 512), bf16...]
where the time goes in v5:
time: 153 us
  Pallas kernels  152 us (99%)
    pallas_call x1, Pallas kernels, per_device(): pl.pallas_call(kernel, out_shape=jax.ShapeDtypeStruct((NR, 64, 512), bf16...  152 us

profile of v5, /device:TPU:1, one launch (start us, length us, event | category | flops | bytes accessed | tf_op | source)
XLA Modules:
  0.0 153.2 jit_solution(10944291080787490942)
XLA Ops:
  0.0 151.6 %shard_map.100 = bf16[32,64,512]{2,1,0:T(8,128)(2,1)S(1)} custom-call(bf16[64,16384]{1,0:T(8,128)(2,1)} %refs_0_.1, f32[2,64,768]{2,1,0:T(8,128)} %refs_1_.1, f32[2,64,768]{2,1,0:T(8,128)} %refs_2_.1, f32[2,64,768]{2,1,0:T(8,128)} %refs_3_.1, f32[2,2048]{1,0:T(2,128)} %refs_4_.1, f32[2,768]{1,0:T(2,128)} %refs_5_.1, f32[2,768]{1,0:T(2,128)} %refs_6_.1, ...), custom_call_target="tpu_custom_call" | custom-call | tf_op jit(solution)/shard_map/pallas_call | solution.py:525
  151.6 1.5 copy.12
